TPU v7x, 32 devices: a whole 2x2x4 slice. The times are simulated.
32 devices in a mesh: sp: 4 (over y, x), tp: 8 (over z, core).
Axes of the slice: x: 2, y: 2, z: 4, core: 2. Of those that a mesh axis runs over, the one named last changes fastest.
Arguments:
- tokens: bfloat16 [2, 512, 4096], P(None, 'sp', 'tp'), may hold values from -6 to 6
- key_matrix: bfloat16 [4096, 4096], P(None, 'tp'), may hold values from -0.09375 to 0.09375
- value_matrix: bfloat16 [4096, 4096], P(None, 'tp'), may hold values from -0.375 to 0.375
- gate_matrix: bfloat16 [4096, 64], replicated, may hold values from -0.09375 to 0.09375
- head_decay_rate: float32 [32], P('tp'), may hold values from 0 to 1, as said below
- extra_log_decay: float32 [2, 32, 512], P(None, 'tp', 'sp'), may hold values from -3 to 0, as said below
- next_token_query: bfloat16 [2, 4096], P(None, 'tp'), may hold values from -6 to 6
- next_token_key: bfloat16 [2, 4096], P(None, 'tp'), may hold values from -6 to 6
- next_token_value: bfloat16 [2, 32, 128], P(None, 'tp', 'sp'), may hold values from -6 to 6
- next_write_strength: float32 [2, 32], P(None, 'tp'), may hold values from 0.05 to 1
- read_norm_gain: float32 [128], P('sp'), may hold values from 0.1 to 1.9
Outputs:
- state_cache: bfloat16 [2, 32, 128, 128], P(None, 'tp', None, 'sp')
- first_read: bfloat16 [2, 32, 128], P(None, 'tp', 'sp')
Inputs may be any that keep to these rules, and one draw needn't show every extreme that they name: `head_decay_rate`: positive. `extra_log_decay`: never positive.
All inputs are finite; a program needn't handle non-finite values.
Results may differ from a plain program's by a relative error of at most 0.013.
Values may be sent and summed in bfloat16 or wider, within the bound.
No kernel may reach another device: no remote copies, remote signals or barrier semaphores. Data moves between devices by JAX's collectives and lax.ppermute only.
A program may use at most 64 MiB of HBM per device.

v0:
```python
import functools

import jax
import jax.numpy as jnp
from jax import lax
from jax.experimental import pallas as pl
from jax.experimental.pallas import tpu as pltpu
from jax.sharding import PartitionSpec as P

DV = 128


exact_mode = lax.Precision.HIGHEST
strength_offset = 5.0


def unit_rows(matrix):
    return matrix * lax.rsqrt(jnp.sum(matrix * matrix, axis=-1, keepdims=True) + 1e-06)


def nilpotent_inverse(mixing):
    extent = mixing.shape[-1]
    result = jnp.zeros_like(mixing) + jnp.eye(extent, dtype=jnp.float32)
    powered = -mixing
    covered = 1
    while covered < extent:
        product = lax.optimization_barrier(
            jnp.einsum("...ij,...jk->...ik", result, powered, precision=exact_mode)
        )
        result = result + product
        powered = jnp.einsum("...ij,...jk->...ik", powered, powered, precision=exact_mode)
        covered = covered * 2
    return result


def block_terms(unit_keys, values, decay_logarithm, strength):
    extent = unit_keys.shape[-2]
    lower = jnp.tril(jnp.ones((extent, extent), jnp.bool_))
    strict = jnp.tril(jnp.ones((extent, extent), jnp.bool_), -1)
    running = jnp.cumsum(decay_logarithm, axis=-1)
    spread = running[..., :, None] - running[..., None, :]
    within = jnp.where(lower, jnp.exp(jnp.where(lower, spread, 0.0)), 0.0)
    scaled = unit_keys * strength[..., None]
    mixing = jnp.where(
        strict,
        jnp.einsum("...id,...jd->...ij", scaled, unit_keys, precision=exact_mode) * within,
        0.0,
    )
    inverse = nilpotent_inverse(mixing)
    writes = jnp.einsum(
        "...ij,...je->...ie", inverse, values * strength[..., None], precision=exact_mode
    )
    erases = jnp.einsum(
        "...ij,...jd->...id", inverse, scaled * jnp.exp(running)[..., None], precision=exact_mode
    )
    final_log = running[..., -1]
    carried = unit_keys * jnp.exp(final_log[..., None] - running)[..., None]
    return (writes, erases, carried, final_log)


def split_blocks(array, block_count):
    shaped = array.reshape(
        array.shape[:2] + (block_count, array.shape[2] // block_count) + array.shape[3:]
    )
    return jnp.moveaxis(shaped, 2, 0)


def local(
    tokens,
    key_matrix,
    value_matrix,
    gate_matrix,
    head_decay_rate,
    extra_log_decay,
    next_token_query,
    next_token_key,
    next_token_value,
    next_write_strength,
    read_norm_gain,
):
    sequences, positions, _ = tokens.shape
    local_heads = head_decay_rate.shape[0]
    key_width = key_matrix.shape[1] // local_heads
    value_width = value_matrix.shape[1] // local_heads
    all_heads = gate_matrix.shape[1] // 2
    group_size = lax.axis_size("sp")
    column_share = value_width // group_size
    first_head = lax.axis_index("tp") * local_heads
    decay_cols = lax.dynamic_slice_in_dim(gate_matrix, first_head, local_heads, 1)
    strength_cols = lax.dynamic_slice_in_dim(gate_matrix, all_heads + first_head, local_heads, 1)
    gate_cols = jnp.concatenate([decay_cols, strength_cols], axis=1)
    row_count = sequences * positions
    incoming = lax.all_gather(tokens, "tp", axis=2, tiled=True)
    span_width = incoming.shape[2]
    flat_rows = incoming.reshape(row_count, span_width)
    products = lax.optimization_barrier(
        (
            jnp.dot(flat_rows, key_matrix, preferred_element_type=jnp.float32),
            jnp.dot(flat_rows, value_matrix, preferred_element_type=jnp.float32),
            jnp.dot(flat_rows, gate_cols, preferred_element_type=jnp.float32),
        )
    )
    key_sum = products[0]
    value_sum = products[1]
    gate_pre = products[2]
    key_float = lax.optimization_barrier(key_sum.astype(jnp.bfloat16)).astype(jnp.float32)
    value_float = lax.optimization_barrier(value_sum.astype(jnp.bfloat16)).astype(jnp.float32)
    unit_keys = unit_rows(
        key_float.reshape(sequences, positions, local_heads, key_width).transpose(0, 2, 1, 3)
    )
    values = value_float.reshape(sequences, positions, local_heads, value_width).transpose(
        0, 2, 1, 3
    )
    gate_projected = gate_pre.reshape(sequences, positions, 2 * local_heads).transpose(0, 2, 1)
    decay_logarithm = (
        -head_decay_rate[None, :, None] * jax.nn.softplus(gate_projected[:, :local_heads])
        + extra_log_decay
    )
    strength = jax.nn.sigmoid(gate_projected[:, local_heads:] - strength_offset)
    block_count = positions // min(64, positions)
    block_parts = block_terms(
        split_blocks(unit_keys, block_count),
        split_blocks(values, block_count),
        split_blocks(decay_logarithm, block_count),
        split_blocks(strength, block_count),
    )
    identity = jnp.zeros((sequences, local_heads, key_width, key_width), jnp.float32) + jnp.eye(
        key_width, dtype=jnp.float32
    )
    start_map = jnp.concatenate(
        [identity, jnp.zeros((sequences, local_heads, key_width, value_width), jnp.float32)],
        axis=-1,
    )

    def advance(current, block_part):
        writes, erases, carried, final_log = block_part
        padded = jnp.concatenate(
            [jnp.zeros(writes.shape[:-1] + (key_width,), jnp.float32), writes], axis=-1
        )
        removed = lax.optimization_barrier(
            jnp.einsum("shcd,shde->shce", erases, current, precision=exact_mode)
        )
        fresh = padded - removed
        added = lax.optimization_barrier(
            jnp.einsum("shcd,shce->shde", carried, fresh, precision=exact_mode)
        )
        current = current * jnp.exp(final_log)[..., None, None] + added
        return (current, None)

    local_map, _ = lax.scan(advance, start_map, block_parts)
    carry_map = local_map[..., :key_width]
    write_map = local_map[..., key_width:]
    carry_copies = jnp.broadcast_to(carry_map[None], (group_size,) + carry_map.shape)
    write_parts = jnp.moveaxis(
        write_map.reshape(sequences, local_heads, key_width, group_size, column_share), 3, 0
    )
    carries = lax.all_to_all(carry_copies, "sp", split_axis=0, concat_axis=0, tiled=True)
    write_cols = lax.all_to_all(write_parts, "sp", split_axis=0, concat_axis=0, tiled=True)

    def fold_step(current, block_map):
        moved = lax.optimization_barrier(
            jnp.einsum("shij,shje->shie", block_map[0], current, precision=exact_mode)
        )
        return (moved + block_map[1], None)

    begin_state = jnp.zeros(write_cols.shape[1:], jnp.float32)
    folded, _ = lax.scan(fold_step, begin_state, (carries, write_cols))
    query_rows = next_token_query.astype(jnp.float32).reshape(sequences, local_heads, key_width)
    unit_new = unit_rows(
        next_token_key.astype(jnp.float32).reshape(sequences, local_heads, key_width)
    )
    value_rows = next_token_value.astype(jnp.float32)
    key_read = jnp.einsum("shd,shde->she", unit_new, folded, precision=exact_mode)
    query_read = jnp.einsum("shd,shde->she", query_rows, folded, precision=exact_mode)
    intersection = jnp.sum(query_rows * unit_new, axis=-1)
    read_raw = query_read + (next_write_strength * intersection)[..., None] * (
        value_rows - key_read
    )
    square_total = lax.psum(jnp.sum(read_raw * read_raw, axis=-1, keepdims=True), "sp")
    first_read = read_raw * lax.rsqrt(square_total / DV + 1e-06) * read_norm_gain
    return (folded.astype(jnp.bfloat16), first_read.astype(jnp.bfloat16))


def split3(value):
    first = value.astype(jnp.bfloat16).astype(jnp.float32)
    rest = value - first
    second = rest.astype(jnp.bfloat16).astype(jnp.float32)
    return first, second, rest - second


def dot_nn(left, right, precision=None):
    return lax.dot_general(
        left, right, (((1,), (0,)), ((), ())), precision=precision, preferred_element_type=jnp.float32
    )


def dot_nt(left, right, precision=None):
    return lax.dot_general(
        left, right, (((1,), (1,)), ((), ())), precision=precision, preferred_element_type=jnp.float32
    )


SIDE = 16
BEGIN_FLOPS, PROJECT_FLOPS, STATE_FLOPS = 4 * 10**9, 2 * 10**9, 4 * 10**9


def source_rows(lane, step, depth):
    me = lax.axis_index("tp")
    owner = (((me // 2) ^ step) * 2) + ((me % 2) ^ lane)
    return pl.ds(pl.multiple_of(owner * depth, depth), depth)


def begin_kernel(rate_ref, value_ref, gain_ref, rate_out, value_out, gain_out):
    place = lax.axis_index("sp")
    heads, width = rate_out.shape
    head_at = lax.broadcasted_iota(jnp.int32, (heads, width), 0)
    rates = jnp.zeros((heads, width), jnp.float32)
    for head in range(heads):
        rates = jnp.where(head_at == head, rate_ref[head], rates)
    rate_out[...] = rates
    columns = gain_ref.shape[1]

    def placed(rows):
        padded = jnp.concatenate(
            [rows, jnp.zeros((rows.shape[0], width - columns), jnp.float32)], axis=1
        )
        return pltpu.roll(padded, place * columns, 1)

    for s in range(value_ref.shape[0]):
        value_out[s] = placed(value_ref[s].astype(jnp.float32))
    gain_out[...] = placed(gain_ref[...])


def partial_kernel(sources, s, *refs):
    pieces, (key_ref, value_ref, gate_ref) = refs[: len(sources)], refs[len(sources) : -2]
    total_ref, gates_ref = refs[-2:]
    positions = total_ref.shape[0]
    width = key_ref.shape[1]
    total_key = total_value = total_gate = 0.0
    for piece, (lane, step) in zip(pieces, sources):
        rows = source_rows(lane, step, piece.shape[1])
        block = piece[...] if step else piece[pl.ds(s * positions, positions), :]
        total_key += dot_nn(block, key_ref[rows, :])
        total_value += dot_nn(block, value_ref[rows, :])
        total_gate += dot_nt(gate_ref[:, rows], block)
    total_ref[:, :width] = total_key
    total_ref[:, width:] = total_value
    gates_ref[...] = total_gate


def project_kernel(sources, s, group, *refs):
    count = len(sources)
    pieces = refs[:count]
    total_ref, gates_ref, key_ref, value_ref, gate_ref = refs[count : count + 5]
    extra_ref, rate_ref, fresh_ref, gain_ref = refs[count + 5 : count + 9]
    outs = refs[count + 9 : count + 9 + group]
    key_sum, value_sum, gate_rows, decay_rows, strength_rows = refs[count + 9 + group :]
    place = lax.axis_index("sp")
    first_head = lax.axis_index("tp") * rate_ref.shape[0]
    heads, positions = extra_ref.shape[1:]
    wide = key_ref.shape[1]
    width = wide // heads
    share = heads // group
    total_key, total_value = total_ref[:, :wide], total_ref[:, wide:]
    total_gate = gates_ref[...]
    for piece, (lane, step) in zip(pieces, sources):
        rows = source_rows(lane, step, piece.shape[1])
        block = piece[...]
        total_key += dot_nn(block, key_ref[rows, :])
        total_value += dot_nn(block, value_ref[rows, :])
        total_gate += dot_nt(gate_ref[:, rows], block)
    gate_rows[...] = total_gate
    half = gate_rows.shape[0] // 2
    gates = [
        jnp.concatenate(
            [gate_rows[pl.ds(start + first_head + head, 1), :] for head in range(heads)], axis=0
        )
        for start in (0, half)
    ]
    key_sum[...] = total_key.astype(jnp.bfloat16)
    value_sum[...] = total_value.astype(jnp.bfloat16)
    row_at = lax.broadcasted_iota(jnp.int32, (positions, positions), 0)
    col_at = lax.broadcasted_iota(jnp.int32, (positions, positions), 1)
    upper = (row_at <= col_at).astype(jnp.bfloat16)
    decay = -rate_ref[...] * jax.nn.softplus(gates[0]) + extra_ref[s]
    parts = jnp.concatenate(split3(decay), axis=0).astype(jnp.bfloat16)
    summed = dot_nn(parts, upper)
    decay_rows[...] = summed[:heads] + summed[heads : 2 * heads] + summed[2 * heads :]
    strength_rows[...] = jax.nn.sigmoid(gates[1] - strength_offset)
    gain_parts = split3(gain_ref[...])
    for m in range(group):
        peer = place ^ m
        for r in range(share):
            head = peer * share + r
            columns = pl.ds(pl.multiple_of(head * width, width), width)
            outs[m][r, pl.ds(0, positions), :] = key_sum[:, columns]
            outs[m][r, pl.ds(positions, positions), :] = value_sum[:, columns]
            side = [
                *split3(decay_rows[pl.ds(head, 1), :]),
                *split3(strength_rows[pl.ds(head, 1), :]),
                fresh_ref[s, pl.ds(head, 1), :],
                *gain_parts,
            ]
            side.append(jnp.zeros((SIDE - len(side), positions), jnp.float32))
            outs[m][r, pl.ds(2 * positions, SIDE), :] = jnp.concatenate(side, axis=0).astype(
                jnp.bfloat16
            )


def halves(value):
    high = value.astype(jnp.bfloat16)
    return high, (value - high.astype(jnp.float32)).astype(jnp.bfloat16)


def dot_wide(left, right):
    left_high, left_low = halves(left)
    right_high, right_low = halves(right)
    columns = right.shape[1]
    both = dot_nn(
        jnp.concatenate([left_high, left_low], axis=1),
        jnp.concatenate(
            [
                jnp.concatenate([right_high, right_low], axis=1),
                jnp.concatenate([right_high, jnp.zeros_like(right_low)], axis=1),
            ],
            axis=0,
        ),
    )
    return both[:, :columns] + both[:, columns:]


def dot_left(left, right):
    return dot_nn(jnp.concatenate(halves(left), axis=1), jnp.concatenate([right, right], axis=0))


def over_unit_lower(lefts, mixings, row_at, col_at):
    extent = mixings[0].shape[0]
    small = 16

    def stacked(tops, bottoms, rights):
        pairs = [
            dot_wide(jnp.concatenate([top, bottom], axis=0), right)
            for top, bottom, right in zip(tops, bottoms, rights)
        ]
        return [pair[:extent] for pair in pairs], [pair[extent:] for pair in pairs]

    def powers(results, steps, covered, reach):
        while 2 * covered < reach:
            gains, squares = stacked(results, steps, steps)
            results = [result + gain for result, gain in zip(results, gains)]
            steps, covered = squares, 2 * covered
        return [result + dot_wide(result, step) for result, step in zip(results, steps)]

    inside = row_at // small == col_at // small
    steps = [jnp.where(inside, -mixing, 0.0) for mixing in mixings]
    eye = (row_at == col_at).astype(jnp.float32)
    diagonals = [eye + step for step in steps]
    diagonals = powers(diagonals, [dot_wide(step, step) for step in steps], 2, small)
    outside = [jnp.where(inside, 0.0, -mixing) for mixing in mixings]
    lefts, steps = stacked(lefts, outside, diagonals)
    return powers(lefts, steps, 1, extent // small)


def state_kernel(s, group, *refs):
    blocks = refs[:group]
    query_ref, new_key_ref, strengths = refs[group : group + 3]
    earlier = refs[group + 3 : -group - 3]
    outs = refs[-group - 3 : -3]
    maps, adds, turned = refs[-3:]
    for m in range(group if earlier else 0):
        outs[m][:s] = earlier[m][...]
    place = lax.axis_index("sp")
    share = blocks[0].shape[0]
    positions = (blocks[0].shape[1] - SIDE) // 2
    width = blocks[0].shape[2]
    row_at = lax.broadcasted_iota(jnp.int32, (positions, positions), 0)
    col_at = lax.broadcasted_iota(jnp.int32, (positions, positions), 1)
    eye = row_at == col_at
    units = [(r, m) for r in range(share) for m in range(group)]
    count = len(units)
    keys = [blocks[m][r, pl.ds(0, positions), :] for r, m in units]
    grams = [dot_nt(key, key) for key in keys]
    values = [blocks[m][r, pl.ds(positions, positions), :] for r, m in units]
    sides = [blocks[m][r, pl.ds(2 * positions, SIDE), :].astype(jnp.float32) for r, m in units]
    decays = [side[0:1] + side[1:2] + side[2:3] for side in sides]
    strength_rows = [side[3:4] + side[4:5] + side[5:6] for side in sides]
    lines = jnp.concatenate([*decays, jnp.zeros((-count % 8, positions), jnp.float32)], axis=0)
    columns = lines.T
    withins = [
        jnp.where(
            row_at > col_at,
            jnp.exp(jnp.where(row_at > col_at, columns[:, u : u + 1] - decays[u], 0.0)),
            0.0,
        )
        for u in range(count)
    ]
    turned_keys = [key.T.astype(jnp.float32) for key in keys]
    squares = [jnp.sum(jnp.where(eye, gram, 0.0), axis=0, keepdims=True) + 1e-06 for gram in grams]
    scales = [lax.rsqrt(square) for square in squares]
    mixings = [
        grams[u] * withins[u] * (strength_rows[u] * scales[u] * scales[u]) for u in range(count)
    ]
    finals = [row[:, positions - 1 :] for row in decays]
    lefts = [
        turned_keys[u] * (strength_rows[u] * scales[u] * scales[u] * jnp.exp(finals[u] - decays[u]))
        for u in range(count)
    ]
    lefts = over_unit_lower(lefts, mixings, row_at, col_at)
    for u, (r, m) in enumerate(units):
        slot = r * group + (place ^ m)
        adds[slot] = dot_left(lefts[u] * (squares[u] * scales[u]), values[u])
        erase = dot_left(lefts[u] * jnp.exp(decays[u]), keys[u])
        maps[slot] = jnp.where(eye, jnp.exp(finals[u]), 0.0) - erase
    for r in range(share):
        level = [(maps[r * group + b], adds[r * group + b]) for b in range(group)]
        while len(level) > 1:
            joined = []
            for b in range(0, len(level), 2):
                (first_map, first_add), (second_map, second_add) = level[b : b + 2]
                if b == 0:
                    joined.append((None, dot_wide(second_map, first_add) + second_add))
                else:
                    both = dot_wide(second_map, jnp.concatenate([first_map, first_add], axis=1))
                    joined.append((both[:, :width], both[:, width:] + second_add))
            level = joined
        state = level[0][1]
        head = place * share + r
        spot = pl.ds(pl.multiple_of(head * width, width), width)
        query = query_ref[:, spot].astype(jnp.float32)[s : s + 1]
        new_key = new_key_ref[:, spot].astype(jnp.float32)[s : s + 1]
        unit_new = new_key * lax.rsqrt(jnp.sum(new_key * new_key, axis=-1, keepdims=True) + 1e-06)
        both = jnp.concatenate([query, unit_new, jnp.zeros((6, width), jnp.float32)], axis=0)
        overlap = jnp.sum(query * unit_new, axis=-1, keepdims=True)
        lane_at = lax.broadcasted_iota(jnp.int32, strengths.shape, 1)
        strength = jnp.sum(jnp.where(lane_at == head, strengths[...], 0.0), axis=1, keepdims=True)
        fresh_row = sum(sides[r * group + m][6:7] for m in range(group))
        gain_row = sum(sides[r * group + m][j : j + 1] for m in range(group) for j in (7, 8, 9))
        reads = dot_wide(both, state)
        raw = reads[0:1] + strength[s : s + 1] * overlap * (fresh_row - reads[1:2])
        first = raw * lax.rsqrt(jnp.mean(raw * raw, axis=-1, keepdims=True) + 1e-06) * gain_row
        turned[...] = state.T.astype(jnp.bfloat16)
        tail = jnp.broadcast_to(first, (SIDE, first.shape[1])).astype(jnp.bfloat16)
        column_share = turned.shape[0] // group
        for m in range(group):
            rows = pl.ds(pl.multiple_of((place ^ m) * column_share, column_share), column_share)
            outs[m][s, r, pl.ds(0, column_share), :] = turned[rows, :]
            outs[m][s, r, pl.ds(column_share, SIDE), :] = tail


def finish_kernel(group, *refs):
    state_ref, read_ref, reads = refs[-3:]
    place = lax.axis_index("sp")
    sequences, share, rows, _ = refs[0].shape
    column_share = rows - SIDE
    for m in range(group):
        part = refs[m]
        for s in range(sequences):
            for r in range(share):
                head = (place ^ m) * share + r
                state_ref[s, head] = part[s, r, pl.ds(0, column_share), :]
                line = pltpu.roll(
                    part[s, r, pl.ds(column_share, SIDE), :].astype(jnp.float32)[:8],
                    (group - place) * column_share,
                    1,
                )
                reads[s, pl.ds(head, 1), :] = line[0:1, :column_share]
    read_ref[...] = reads[...].astype(jnp.bfloat16)


def fast_local(
    tokens,
    key_matrix,
    value_matrix,
    gate_matrix,
    head_decay_rate,
    extra_log_decay,
    next_token_query,
    next_token_key,
    next_token_value,
    next_write_strength,
    read_norm_gain,
):
    sequences, positions, depth = tokens.shape
    heads = head_decay_rate.shape[0]
    group = lax.axis_size("sp")
    members = lax.axis_size("tp")
    share = heads // group
    width = key_matrix.shape[1] // heads
    column_share = next_token_value.shape[2]
    value_width = column_share * group
    f32, bf16 = jnp.float32, jnp.bfloat16

    def over_tp(array, step):
        links = [(z * 2 + c, (z ^ step) * 2 + c) for z in range(members // 2) for c in range(2)]
        return lax.ppermute(array, "tp", links)

    def to_partner(array):
        return lax.ppermute(array, "tp", [(i, i ^ 1) for i in range(members)])

    def over_sp(array, step):
        return lax.ppermute(array, "sp", [(i, i ^ step) for i in range(group)])

    def after_all(array, *others):
        return lax.optimization_barrier((array, others))[0]

    def kernel(body, mib, flops, shapes, scratch, operands, specs=None):
        return pl.pallas_call(
            body,
            out_shape=[jax.ShapeDtypeStruct(*shape) for shape in shapes],
            in_specs=specs or [vmem] * len(operands),
            out_specs=[vmem] * len(shapes),
            scratch_shapes=scratch,
            compiler_params=pltpu.CompilerParams(vmem_limit_bytes=mib * 2**20),
            cost_estimate=pl.CostEstimate(flops=flops, bytes_accessed=0, transcendentals=0),
        )(*operands)

    vmem = pl.BlockSpec(memory_space=pltpu.VMEM)
    own = tokens.reshape(sequences * positions, depth)
    rows, out_rows = 2 * positions + SIDE, column_share + SIDE
    steps = range(1, members // 2)
    pairs = [(lane, step) for step in steps for lane in (0, 1)]
    got = [[over_tp(tokens[s], step) for step in steps] for s in range(sequences)]
    wide = key_matrix.shape[1]
    partner = to_partner(own)
    begun = kernel(
        begin_kernel,
        4,
        BEGIN_FLOPS,
        [
            ((heads, positions), f32),
            ((sequences, heads, value_width), f32),
            ((1, value_width), f32),
        ],
        [],
        [head_decay_rate, next_token_value, read_norm_gain[None]],
        [pl.BlockSpec(memory_space=pltpu.SMEM), vmem, vmem],
    )
    blocks, after = [], tuple(begun)
    for s in range(sequences):
        arrived = []
        for step, piece in zip(steps, got[s]):
            piece = after_all(piece, *(begun if step == steps[0] else after))
            arrived += [piece, to_partner(piece)]
        early = len(arrived) - 4
        weights = [key_matrix, value_matrix, gate_matrix.T]
        totals = kernel(
            functools.partial(partial_kernel, [(0, 0), (1, 0), *pairs[:early]], s),
            12,
            PROJECT_FLOPS,
            [((positions, 2 * wide), f32), ((gate_matrix.shape[1], positions), f32)],
            [],
            [own, partner, *arrived[:early], *weights],
        )
        messages = kernel(
            functools.partial(project_kernel, pairs[early:], s, group),
            12,
            PROJECT_FLOPS,
            [((share, rows, width), bf16)] * group,
            [
                pltpu.VMEM((positions, wide), bf16),
                pltpu.VMEM((positions, wide), bf16),
                pltpu.VMEM((gate_matrix.shape[1], positions), f32),
                pltpu.VMEM((heads, positions), f32),
                pltpu.VMEM((heads, positions), f32),
            ],
            [
                *arrived[early:],
                *totals,
                *weights,
                extra_log_decay,
                *begun,
            ],
        )
        after = tuple(messages)
        blocks.append([messages[0]] + [over_sp(messages[m], m) for m in range(1, group)])
    results = []
    for s in range(sequences):
        results = kernel(
            functools.partial(state_kernel, s, group),
            8,
            STATE_FLOPS,
            [((s + 1, share, out_rows, width), bf16)] * group,
            [
                pltpu.VMEM((heads, width, value_width), f32),
                pltpu.VMEM((heads, width, width), f32),
                pltpu.VMEM((value_width, width), bf16),
            ],
            [*blocks[s], next_token_query, next_token_key, next_write_strength, *results],
        )
    parts = [results[0]] + [over_sp(results[m], m) for m in range(1, group)]
    turned_state, first_read = kernel(
        functools.partial(finish_kernel, group),
        4,
        10**6,
        [((sequences, heads, column_share, width), bf16), ((sequences, heads, column_share), bf16)],
        [pltpu.VMEM((sequences, heads, column_share), f32)],
        parts,
    )
    return turned_state.transpose(0, 1, 3, 2), first_read


def pick(mesh):
    def body(*args):
        group, members = mesh.shape["sp"], mesh.shape["tp"]
        tokens, heads = args[0], args[4].shape[0]
        powers = group & (group - 1) == 0 and members & (members - 1) == 0
        square = args[1].shape[1] // heads == tokens.shape[1] == args[2].shape[1] // heads
        if powers and members > 1 and heads % group == 0 and square:
            return fast_local(*args)
        return local(*args)

    return body


def solution(mesh):
    in_specs = (
        P(None, "sp", "tp"),
        P(None, "tp"),
        P(None, "tp"),
        P(),
        P("tp"),
        P(None, "tp", "sp"),
        P(None, "tp"),
        P(None, "tp"),
        P(None, "tp", "sp"),
        P(None, "tp"),
        P("sp"),
    )
    out_specs = (P(None, "tp", None, "sp"), P(None, "tp", "sp"))
    return jax.shard_map(
        pick(mesh), mesh=mesh, in_specs=in_specs, out_specs=out_specs, check_vma=False)
```

profile of v0, /device:TPU:0, one launch (start us, length us, event | category | flops | bytes accessed | tf_op | source)
XLA Modules:
  0.0 52.5 jit_solution(4765438656919404348)
XLA Ops:
  0.6 1.0 %slice_bitcast_fusion = (bf16[128,512]{1,0:T(8,128)(2,1)S(1)}, bf16[128,512]{1,0:T(8,128)(2,1)S(1)}) fusion(bf16[2,128,512]{2,1,0:T(8,128)(2,1)} %param.11), kind=kLoop, calls=%fused_computation | loop fusion | bytes 524288 | tf_op jit(solution)/shard_map/squeeze | solution.py:522
  1.6 3.1 %collective-permute-start.6 = (bf16[128,512]{1,0:T(8,128)(2,1)S(1)}, bf16[128,512]{1,0:T(8,128)(2,1)S(1)}, u32[]{:S(2)}, u32[]{:S(2)}) collective-permute-start(bf16[128,512]{1,0:T(8,128)(2,1)S(1)} %get-tuple-element.64), channel_id=1, source_target_pairs={{0,2},{1,3},{2,0},{3,1},{4,6},{5,7},{6,4},{7,5},{8,10},{9,11},{10,... | collective-permute-start | bytes 393224 | tf_op jit(solution)/shard_map/ppermute | solution.py:495
  4.7 2.6 %collective-permute-start.1 = (bf16[128,512]{1,0:T(8,128)(2,1)S(1)}, bf16[128,512]{1,0:T(8,128)(2,1)S(1)}, u32[]{:S(2)}, u32[]{:S(2)}) collective-permute-start(bf16[128,512]{1,0:T(8,128)(2,1)S(1)} %get-tuple-element.64), channel_id=1, source_target_pairs={{0,4},{1,5},{2,6},{3,7},{4,0},{5,1},{6,2},{7,3},{8,12},{9,13},{10,... | collective-permute-start | bytes 393224 | tf_op jit(solution)/shard_map/ppermute | solution.py:495
  7.3 0.0 collective-permute-start.3
  7.3 0.0 collective-permute-start.5
  7.3 0.9 %collective-permute-start.11 = (bf16[128,512]{1,0:T(8,128)(2,1)S(1)}, bf16[128,512]{1,0:T(8,128)(2,1)S(1)}, u32[]{:S(2)}, u32[]{:S(2)}) collective-permute-start(bf16[128,512]{1,0:T(8,128)(2,1)S(1)} %get-tuple-element.65), channel_id=1, source_target_pairs={{0,2},{1,3},{2,0},{3,1},{4,6},{5,7},{6,4},{7,5},{8,10},{9,11},{10,... | collective-permute-start | bytes 393224 | tf_op jit(solution)/shard_map/ppermute | solution.py:495
  8.2 0.7 %copy-done.5 = bf16[2,4,32]{2,1,0:T(4,128)(2,1)S(1)} copy-done((bf16[2,4,32]{2,1,0:T(4,128)(2,1)S(1)}, bf16[2,4,32]{2,1,0:T(4,128)(2,1)}, u32[]{:S(2)}) %copy-start.5) | copy-done | bytes 536
  8.9 0.7 %copy-done.9 = f32[4]{0:T(128)S(1)} copy-done((f32[4]{0:T(128)S(1)}, f32[4]{0:T(128)}, u32[]{:S(2)}) %copy-start.9) | copy-done | bytes 40
  9.6 0.7 %copy-done.10 = f32[32]{0:T(128)S(1)} copy-done((f32[32]{0:T(128)S(1)}, f32[32]{0:T(128)}, u32[]{:S(2)}) %copy-start.10) | copy-done | bytes 152
  10.2 0.6 %shard_map.122 = (f32[4,128]{1,0:T(4,128)S(1)}, f32[2,4,128]{2,1,0:T(4,128)S(1)}, f32[1,128]{1,0:T(1,128)S(1)}) custom-call(f32[4]{0:T(128)S(1)} %copy-done.9, bf16[2,4,32]{2,1,0:T(4,128)(2,1)S(1)} %copy-done.5, f32[1,32]{1,0:T(1,128)S(1)} %bitcast.15), custom_call_target="tpu_custom_call" | custom-call | flops 4000000000 | tf_op jit(solution)/shard_map/pallas_call | solution.py:507
  10.9 0.0 collective-permute-done.6.refs_2_
  10.9 0.2 collective-permute-start.7
  11.1 6.5 %collective-permute-done.1.refs_0_ = bf16[128,512]{1,0:T(8,128)(2,1)S(1)} collective-permute-done((bf16[128,512]{1,0:T(8,128)(2,1)S(1)}, bf16[128,512]{1,0:T(8,128)(2,1)S(1)}, u32[]{:S(2)}, u32[]{:S(2)}) %collective-permute-start.1) | collective-permute-done | bytes 131104 | tf_op jit(solution)/shard_map/ppermute | solution.py:495
  17.6 2.3 %collective-permute-start.9 = (bf16[128,512]{1,0:T(8,128)(2,1)S(1)}, bf16[128,512]{1,0:T(8,128)(2,1)S(1)}, u32[]{:S(2)}, u32[]{:S(2)}) collective-permute-start(bf16[128,512]{1,0:T(8,128)(2,1)S(1)} %get-tuple-element.65), channel_id=1, source_target_pairs={{0,6},{1,7},{2,4},{3,5},{4,2},{5,3},{6,0},{7,1},{8,14},{9,15},{10,... | collective-permute-start | bytes 393224 | tf_op jit(solution)/shard_map/ppermute | solution.py:495
  19.9 6.1 %collective-permute-start = (bf16[128,512]{1,0:T(8,128)(2,1)S(1)}, bf16[128,512]{1,0:T(8,128)(2,1)S(1)}, u32[]{:S(2)}, u32[]{:S(2)}) collective-permute-start(bf16[128,512]{1,0:T(8,128)(2,1)S(1)} %get-tuple-element.65), channel_id=1, source_target_pairs={{0,4},{1,5},{2,6},{3,7},{4,0},{5,1},{6,2},{7,3},{8,12},{9,13},{10,... | collective-permute-start | bytes 393224 | tf_op jit(solution)/shard_map/ppermute | solution.py:495
  26.1 0.0 collective-permute-done.11.refs_2_
  26.1 0.0 collective-permute-start.2
  26.1 0.0 collective-permute-done.7.refs_3_
  26.1 0.5 collective-permute-start.4
  26.6 0.0 collective-permute-done.5.refs_1_
  26.6 0.1 collective-permute-start.12
  26.7 0.0 copy-start.4
  26.7 0.9 %shard_map.123 = (f32[128,1024]{1,0:T(8,128)S(1)}, f32[64,128]{1,0:T(8,128)S(1)}) custom-call(bf16[256,512]{1,0:T(8,128)(2,1)S(1)} %bitcast.13, bf16[256,512]{1,0:T(8,128)(2,1)S(1)} %collective-permute-done.5.refs_1_, bf16[128,512]{1,0:T(8,128)(2,1)S(1)} %collective-permute-done.6.refs_2_, bf16[128,512]{1,0:T(8,128)(2,1)S(1)} %collective-permute-done.7.refs_3_, ...), custom_call_target="tpu_custom_call" | custom-call | flops 2000000000 | tf_op jit(solution)/shard_map/pallas_call | solution.py:507
  27.6 0.0 collective-permute-done.4.refs_3_
  27.6 1.1 %shard_map.124 = (bf16[1,272,128]{2,1,0:T(8,128)(2,1)S(1)}, bf16[1,272,128]{2,1,0:T(8,128)(2,1)S(1)}, bf16[1,272,128]{2,1,0:T(8,128)(2,1)S(1)}, bf16[1,272,128]{2,1,0:T(8,128)(2,1)S(1)}) custom-call(bf16[128,512]{1,0:T(8,128)(2,1)S(1)} %collective-permute-done.1.refs_0_, bf16[128,512]{1,0:T(8,128)(2,1)S(1)} %collective-permute-done.2.refs_1_, ...), custom_call_target="tpu_custom_call" | custom-call | flops 2000000000 | tf_op jit(solution)/shard_map/pallas_call | solution.py:507
  28.7 1.6 %collective-permute-start.16 = (bf16[1,272,128]{2,1,0:T(8,128)(2,1)S(1)}, bf16[1,272,128]{2,1,0:T(8,128)(2,1)S(1)}, u32[]{:S(2)}, u32[]{:S(2)}) collective-permute-start(bf16[1,272,128]{2,1,0:T(8,128)(2,1)S(1)} %get-tuple-element.42), channel_id=1, source_target_pairs={{0,8},{8,0},{16,24},{24,16},{1,9},{9,1},{17,25},{25,17},{2,10},{10... | collective-permute-start | bytes 208904 | tf_op jit(solution)/shard_map/ppermute | solution.py:501
  30.3 1.5 %collective-permute-start.17 = (bf16[1,272,128]{2,1,0:T(8,128)(2,1)S(1)}, bf16[1,272,128]{2,1,0:T(8,128)(2,1)S(1)}, u32[]{:S(2)}, u32[]{:S(2)}) collective-permute-start(bf16[1,272,128]{2,1,0:T(8,128)(2,1)S(1)} %get-tuple-element.43), channel_id=1, source_target_pairs={{0,16},{8,24},{16,0},{24,8},{1,17},{9,25},{17,1},{25,9},{2,18},{10... | collective-permute-start | bytes 208904 | tf_op jit(solution)/shard_map/ppermute | solution.py:501
  31.8 0.5 collective-permute-start.18
  32.3 0.0 collective-permute-done.refs_0_
  32.3 0.0 collective-permute-start.10
  32.3 0.5 collective-permute-start.8
  32.8 0.9 %shard_map.125 = (f32[128,1024]{1,0:T(8,128)S(1)}, f32[64,128]{1,0:T(8,128)S(1)}) custom-call(bf16[256,512]{1,0:T(8,128)(2,1)S(1)} %bitcast.14, bf16[256,512]{1,0:T(8,128)(2,1)S(1)} %collective-permute-done.5.refs_1_, bf16[128,512]{1,0:T(8,128)(2,1)S(1)} %collective-permute-done.11.refs_2_, bf16[128,512]{1,0:T(8,128)(2,1)S(1)} %collective-permute-done.12.refs_3_, ...), custom_call_target="tpu_custom_call" | custom-call | flops 2000000000 | tf_op jit(solution)/shard_map/pallas_call | solution.py:507
  33.7 0.1 collective-permute-done.8.refs_1_
  33.9 1.1 %shard_map.126 = (bf16[1,272,128]{2,1,0:T(8,128)(2,1)S(1)}, bf16[1,272,128]{2,1,0:T(8,128)(2,1)S(1)}, bf16[1,272,128]{2,1,0:T(8,128)(2,1)S(1)}, bf16[1,272,128]{2,1,0:T(8,128)(2,1)S(1)}) custom-call(bf16[128,512]{1,0:T(8,128)(2,1)S(1)} %collective-permute-done.refs_0_, bf16[128,512]{1,0:T(8,128)(2,1)S(1)} %collective-permute-done.8.refs_1_, ...), custom_call_target="tpu_custom_call" | custom-call | flops 2000000000 | tf_op jit(solution)/shard_map/pallas_call | solution.py:507
  35.0 1.6 %collective-permute-start.13 = (bf16[1,272,128]{2,1,0:T(8,128)(2,1)S(1)}, bf16[1,272,128]{2,1,0:T(8,128)(2,1)S(1)}, u32[]{:S(2)}, u32[]{:S(2)}) collective-permute-start(bf16[1,272,128]{2,1,0:T(8,128)(2,1)S(1)} %get-tuple-element.51), channel_id=1, source_target_pairs={{0,8},{8,0},{16,24},{24,16},{1,9},{9,1},{17,25},{25,17},{2,10},{10... | collective-permute-start | bytes 208904 | tf_op jit(solution)/shard_map/ppermute | solution.py:501
  36.5 1.5 %collective-permute-start.14 = (bf16[1,272,128]{2,1,0:T(8,128)(2,1)S(1)}, bf16[1,272,128]{2,1,0:T(8,128)(2,1)S(1)}, u32[]{:S(2)}, u32[]{:S(2)}) collective-permute-start(bf16[1,272,128]{2,1,0:T(8,128)(2,1)S(1)} %get-tuple-element.52), channel_id=1, source_target_pairs={{0,16},{8,24},{16,0},{24,8},{1,17},{9,25},{17,1},{25,9},{2,18},{10... | collective-permute-start | bytes 208904 | tf_op jit(solution)/shard_map/ppermute | solution.py:501
  38.0 0.5 collective-permute-start.15
  38.6 2.7 %shard_map.127 = (bf16[1,1,48,128]{3,2,1,0:T(8,128)(2,1)S(1)}, bf16[1,1,48,128]{3,2,1,0:T(8,128)(2,1)S(1)}, bf16[1,1,48,128]{3,2,1,0:T(8,128)(2,1)S(1)}, bf16[1,1,48,128]{3,2,1,0:T(8,128)(2,1)S(1)}) custom-call(bf16[1,272,128]{2,1,0:T(8,128)(2,1)S(1)} %get-tuple-element.41.refs_0_, bf16[1,272,128]{2,1,0:T(8,128)(2,1)S(1)} %collective-permute-done.16.refs_1_, ...), custom_call_target="tpu_custom_call" | custom-call | flops 4000000000 | tf_op jit(solution)/shard_map/pallas_call | solution.py:507
  41.3 0.0 collective-permute-done.14.refs_2_
  41.3 1.9 %collective-permute-done.15.refs_3_ = bf16[1,272,128]{2,1,0:T(8,128)(2,1)S(1)} collective-permute-done((bf16[1,272,128]{2,1,0:T(8,128)(2,1)S(1)}, bf16[1,272,128]{2,1,0:T(8,128)(2,1)S(1)}, u32[]{:S(2)}, u32[]{:S(2)}) %collective-permute-start.15) | collective-permute-done | bytes 69664 | tf_op jit(solution)/shard_map/ppermute | solution.py:501
  43.2 2.7 %shard_map.128 = (bf16[2,1,48,128]{3,2,1,0:T(8,128)(2,1)S(1)}, bf16[2,1,48,128]{3,2,1,0:T(8,128)(2,1)S(1)}, bf16[2,1,48,128]{3,2,1,0:T(8,128)(2,1)S(1)}, bf16[2,1,48,128]{3,2,1,0:T(8,128)(2,1)S(1)}) custom-call(bf16[1,272,128]{2,1,0:T(8,128)(2,1)S(1)} %get-tuple-element.50.refs_0_, bf16[1,272,128]{2,1,0:T(8,128)(2,1)S(1)} %collective-permute-done.13.refs_1_, ...), custom_call_target="tpu_custom_call" | custom-call | flops 4000000000 | tf_op jit(solution)/shard_map/pallas_call | solution.py:507
  46.0 0.6 %collective-permute-start.19 = (bf16[2,1,48,128]{3,2,1,0:T(8,128)(2,1)S(1)}, bf16[2,1,48,128]{3,2,1,0:T(8,128)(2,1)S(1)}, u32[]{:S(2)}, u32[]{:S(2)}) collective-permute-start(bf16[2,1,48,128]{3,2,1,0:T(8,128)(2,1)S(1)} %get-tuple-element.59), channel_id=1, source_target_pairs={{0,8},{8,0},{16,24},{24,16},{1,9},{9,1},{17,25},{25,17},{2,10},{10... | collective-permute-start | bytes 73736 | tf_op jit(solution)/shard_map/ppermute | solution.py:501
  46.5 0.6 %collective-permute-start.20 = (bf16[2,1,48,128]{3,2,1,0:T(8,128)(2,1)S(1)}, bf16[2,1,48,128]{3,2,1,0:T(8,128)(2,1)S(1)}, u32[]{:S(2)}, u32[]{:S(2)}) collective-permute-start(bf16[2,1,48,128]{3,2,1,0:T(8,128)(2,1)S(1)} %get-tuple-element.60), channel_id=1, source_target_pairs={{0,16},{8,24},{16,0},{24,8},{1,17},{9,25},{17,1},{25,9},{2,18},{10... | collective-permute-start | bytes 73736 | tf_op jit(solution)/shard_map/ppermute | solution.py:501
  47.1 2.4 %collective-permute-start.21 = (bf16[2,1,48,128]{3,2,1,0:T(8,128)(2,1)S(1)}, bf16[2,1,48,128]{3,2,1,0:T(8,128)(2,1)S(1)}, u32[]{:S(2)}, u32[]{:S(2)}) collective-permute-start(bf16[2,1,48,128]{3,2,1,0:T(8,128)(2,1)S(1)} %get-tuple-element.61), channel_id=1, source_target_pairs={{0,24},{8,16},{16,8},{24,0},{1,25},{9,17},{17,9},{25,1},{2,26},{10... | collective-permute-start | bytes 73736 | tf_op jit(solution)/shard_map/ppermute | solution.py:501
  49.5 0.3 collective-permute-done.19.refs_1_
  49.8 0.5 %collective-permute-done.20.refs_2_ = bf16[2,1,48,128]{3,2,1,0:T(8,128)(2,1)S(1)} collective-permute-done((bf16[2,1,48,128]{3,2,1,0:T(8,128)(2,1)S(1)}, bf16[2,1,48,128]{3,2,1,0:T(8,128)(2,1)S(1)}, u32[]{:S(2)}, u32[]{:S(2)}) %collective-permute-start.20) | collective-permute-done | bytes 24608 | tf_op jit(solution)/shard_map/ppermute | solution.py:501
  50.3 1.5 %collective-permute-done.21.refs_3_ = bf16[2,1,48,128]{3,2,1,0:T(8,128)(2,1)S(1)} collective-permute-done((bf16[2,1,48,128]{3,2,1,0:T(8,128)(2,1)S(1)}, bf16[2,1,48,128]{3,2,1,0:T(8,128)(2,1)S(1)}, u32[]{:S(2)}, u32[]{:S(2)}) %collective-permute-start.21) | collective-permute-done | bytes 24608 | tf_op jit(solution)/shard_map/ppermute | solution.py:501
  51.8 0.7 %shard_map.129 = (bf16[2,4,32,128]{3,2,1,0:T(8,128)(2,1)}, bf16[2,4,32]{2,1,0:T(4,128)(2,1)}) custom-call(bf16[2,1,48,128]{3,2,1,0:T(8,128)(2,1)S(1)} %get-tuple-element.58.refs_0_, bf16[2,1,48,128]{3,2,1,0:T(8,128)(2,1)S(1)} %collective-permute-done.19.refs_1_, bf16[2,1,48,128]{3,2,1,0:T(8,128)(2,1)S(1)} %collective-permute-done.20.refs_2_, ...), custom_call_target="tpu_custom_call" | custom-call | flops 1000000 | tf_op jit(solution)/shard_map/pallas_call | solution.py:507
  (27 shorter events, 0.1 us)
Async XLA Ops:
  1.6 9.2 %collective-permute-start.6 = (bf16[128,512]{1,0:T(8,128)(2,1)S(1)}, bf16[128,512]{1,0:T(8,128)(2,1)S(1)}, u32[]{:S(2)}, u32[]{:S(2)}) collective-permute-start(bf16[128,512]{1,0:T(8,128)(2,1)S(1)} %get-tuple-element.64), channel_id=1, source_target_pairs={{0,2},{1,3},{2,0},{3,1},{4,6},{5,7},{6,4},{7,5},{8,10},{9,11},{10,... | collective-permute-start | bytes 393224 | tf_op jit(solution)/shard_map/ppermute | solution.py:495
  4.7 12.9 %collective-permute-start.1 = (bf16[128,512]{1,0:T(8,128)(2,1)S(1)}, bf16[128,512]{1,0:T(8,128)(2,1)S(1)}, u32[]{:S(2)}, u32[]{:S(2)}) collective-permute-start(bf16[128,512]{1,0:T(8,128)(2,1)S(1)} %get-tuple-element.64), channel_id=1, source_target_pairs={{0,4},{1,5},{2,6},{3,7},{4,0},{5,1},{6,2},{7,3},{8,12},{9,13},{10,... | collective-permute-start | bytes 393224 | tf_op jit(solution)/shard_map/ppermute | solution.py:495
  7.3 12.6 %collective-permute-start.3 = (bf16[128,512]{1,0:T(8,128)(2,1)S(1)}, bf16[128,512]{1,0:T(8,128)(2,1)S(1)}, u32[]{:S(2)}, u32[]{:S(2)}) collective-permute-start(bf16[128,512]{1,0:T(8,128)(2,1)S(1)} %get-tuple-element.64), channel_id=1, source_target_pairs={{0,6},{1,7},{2,4},{3,5},{4,2},{5,3},{6,0},{7,1},{8,14},{9,15},{10,... | collective-permute-start | bytes 393224 | tf_op jit(solution)/shard_map/ppermute | solution.py:495
  7.3 19.3 %collective-permute-start.5 = (bf16[256,512]{1,0:T(8,128)(2,1)}, bf16[256,512]{1,0:T(8,128)(2,1)S(1)}, u32[]{:S(2)}, u32[]{:S(2)}) collective-permute-start(bf16[256,512]{1,0:T(8,128)(2,1)} %bitcast.12), channel_id=1, source_target_pairs={{0,1},{1,0},{2,3},{3,2},{4,5},{5,4},{6,7},{7,6},{8,9},{9,8},{10,11... | collective-permute-start | bytes 786440 | tf_op jit(solution)/shard_map/ppermute | solution.py:498
  7.3 18.7 %collective-permute-start.11 = (bf16[128,512]{1,0:T(8,128)(2,1)S(1)}, bf16[128,512]{1,0:T(8,128)(2,1)S(1)}, u32[]{:S(2)}, u32[]{:S(2)}) collective-permute-start(bf16[128,512]{1,0:T(8,128)(2,1)S(1)} %get-tuple-element.65), channel_id=1, source_target_pairs={{0,2},{1,3},{2,0},{3,1},{4,6},{5,7},{6,4},{7,5},{8,10},{9,11},{10,... | collective-permute-start | bytes 393224 | tf_op jit(solution)/shard_map/ppermute | solution.py:495
  8.2 0.7 %copy-start.5 = (bf16[2,4,32]{2,1,0:T(4,128)(2,1)S(1)}, bf16[2,4,32]{2,1,0:T(4,128)(2,1)}, u32[]{:S(2)}) copy-start(bf16[2,4,32]{2,1,0:T(4,128)(2,1)} %value_ref.1) | copy-start | bytes 1540
  8.9 0.7 %copy-start.9 = (f32[4]{0:T(128)S(1)}, f32[4]{0:T(128)}, u32[]{:S(2)}) copy-start(f32[4]{0:T(128)} %rate_ref.1) | copy-start | bytes 52
  9.6 0.7 %copy-start.10 = (f32[32]{0:T(128)S(1)}, f32[32]{0:T(128)}, u32[]{:S(2)}) copy-start(f32[32]{0:T(128)} %param.21) | copy-start | bytes 388
  10.2 16.4 %copy-start = (bf16[4096,512]{1,0:T(8,128)(2,1)S(1)}, bf16[4096,512]{1,0:T(8,128)(2,1)}, u32[]{:S(2)}) copy-start(bf16[4096,512]{1,0:T(8,128)(2,1)} %refs_6_.5) | copy-start | bytes 12582916
  10.2 16.4 %copy-start.1 = (bf16[4096,512]{1,0:T(8,128)(2,1)S(1)}, bf16[4096,512]{1,0:T(8,128)(2,1)}, u32[]{:S(2)}) copy-start(bf16[4096,512]{1,0:T(8,128)(2,1)} %refs_7_.3) | copy-start | bytes 12582916
  10.2 16.4 %copy-start.2 = (bf16[4096,64]{0,1:T(8,128)(2,1)S(1)}, bf16[4096,64]{0,1:T(8,128)(2,1)}, u32[]{:S(2)}) copy-start(bf16[4096,64]{0,1:T(8,128)(2,1)} %param.14) | copy-start | bytes 1572868
  10.2 16.4 %copy-start.3 = (bf16[2,128,512]{2,1,0:T(8,128)(2,1)S(1)}, bf16[2,128,512]{2,1,0:T(8,128)(2,1)}, u32[]{:S(2)}) copy-start(bf16[2,128,512]{2,1,0:T(8,128)(2,1)} %param.11) | copy-start | bytes 786436
  10.9 15.2 %collective-permute-start.7 = (bf16[128,512]{1,0:T(8,128)(2,1)S(1)}, bf16[128,512]{1,0:T(8,128)(2,1)S(1)}, u32[]{:S(2)}, u32[]{:S(2)}) collective-permute-start(bf16[128,512]{1,0:T(8,128)(2,1)S(1)} %collective-permute-done.6.refs_2_), channel_id=1, source_target_pairs={{0,1},{1,0},{2,3},{3,2},{4,5},{5,4},{6,7},{7,6},{8,9},{9,8},{10,11... | collective-permute-start | bytes 393224 | tf_op jit(solution)/shard_map/ppermute | solution.py:498
  17.6 14.2 %collective-permute-start.9 = (bf16[128,512]{1,0:T(8,128)(2,1)S(1)}, bf16[128,512]{1,0:T(8,128)(2,1)S(1)}, u32[]{:S(2)}, u32[]{:S(2)}) collective-permute-start(bf16[128,512]{1,0:T(8,128)(2,1)S(1)} %get-tuple-element.65), channel_id=1, source_target_pairs={{0,6},{1,7},{2,4},{3,5},{4,2},{5,3},{6,0},{7,1},{8,14},{9,15},{10,... | collective-permute-start | bytes 393224 | tf_op jit(solution)/shard_map/ppermute | solution.py:495
  19.9 12.4 %collective-permute-start = (bf16[128,512]{1,0:T(8,128)(2,1)S(1)}, bf16[128,512]{1,0:T(8,128)(2,1)S(1)}, u32[]{:S(2)}, u32[]{:S(2)}) collective-permute-start(bf16[128,512]{1,0:T(8,128)(2,1)S(1)} %get-tuple-element.65), channel_id=1, source_target_pairs={{0,4},{1,5},{2,6},{3,7},{4,0},{5,1},{6,2},{7,3},{8,12},{9,13},{10,... | collective-permute-start | bytes 393224 | tf_op jit(solution)/shard_map/ppermute | solution.py:495
  26.1 1.5 %collective-permute-start.2 = (bf16[128,512]{1,0:T(8,128)(2,1)S(1)}, bf16[128,512]{1,0:T(8,128)(2,1)S(1)}, u32[]{:S(2)}, u32[]{:S(2)}) collective-permute-start(bf16[128,512]{1,0:T(8,128)(2,1)S(1)} %collective-permute-done.1.refs_0_), channel_id=1, source_target_pairs={{0,1},{1,0},{2,3},{3,2},{4,5},{5,4},{6,7},{7,6},{8,9},{9,8},{10,11... | collective-permute-start | bytes 393224 | tf_op jit(solution)/shard_map/ppermute | solution.py:498
  26.1 1.5 %collective-permute-start.4 = (bf16[128,512]{1,0:T(8,128)(2,1)S(1)}, bf16[128,512]{1,0:T(8,128)(2,1)S(1)}, u32[]{:S(2)}, u32[]{:S(2)}) collective-permute-start(bf16[128,512]{1,0:T(8,128)(2,1)S(1)} %collective-permute-done.3.refs_2_), channel_id=1, source_target_pairs={{0,1},{1,0},{2,3},{3,2},{4,5},{5,4},{6,7},{7,6},{8,9},{9,8},{10,11... | collective-permute-start | bytes 393224 | tf_op jit(solution)/shard_map/ppermute | solution.py:498
  26.6 5.7 %collective-permute-start.12 = (bf16[128,512]{1,0:T(8,128)(2,1)S(1)}, bf16[128,512]{1,0:T(8,128)(2,1)S(1)}, u32[]{:S(2)}, u32[]{:S(2)}) collective-permute-start(bf16[128,512]{1,0:T(8,128)(2,1)S(1)} %collective-permute-done.11.refs_2_), channel_id=1, source_target_pairs={{0,1},{1,0},{2,3},{3,2},{4,5},{5,4},{6,7},{7,6},{8,9},{9,8},{10,11... | collective-permute-start | bytes 393224 | tf_op jit(solution)/shard_map/ppermute | solution.py:498
  26.7 0.9 %copy-start.4 = (f32[2,4,128]{2,1,0:T(4,128)S(1)}, f32[2,4,128]{2,1,0:T(4,128)}, u32[]{:S(2)}) copy-start(f32[2,4,128]{2,1,0:T(4,128)} %refs_9_.3) | copy-start | bytes 12292
  28.7 9.3 %collective-permute-start.16 = (bf16[1,272,128]{2,1,0:T(8,128)(2,1)S(1)}, bf16[1,272,128]{2,1,0:T(8,128)(2,1)S(1)}, u32[]{:S(2)}, u32[]{:S(2)}) collective-permute-start(bf16[1,272,128]{2,1,0:T(8,128)(2,1)S(1)} %get-tuple-element.42), channel_id=1, source_target_pairs={{0,8},{8,0},{16,24},{24,16},{1,9},{9,1},{17,25},{25,17},{2,10},{10... | collective-permute-start | bytes 208904 | tf_op jit(solution)/shard_map/ppermute | solution.py:501
  30.3 8.2 %collective-permute-start.17 = (bf16[1,272,128]{2,1,0:T(8,128)(2,1)S(1)}, bf16[1,272,128]{2,1,0:T(8,128)(2,1)S(1)}, u32[]{:S(2)}, u32[]{:S(2)}) collective-permute-start(bf16[1,272,128]{2,1,0:T(8,128)(2,1)S(1)} %get-tuple-element.43), channel_id=1, source_target_pairs={{0,16},{8,24},{16,0},{24,8},{1,17},{9,25},{17,1},{25,9},{2,18},{10... | collective-permute-start | bytes 208904 | tf_op jit(solution)/shard_map/ppermute | solution.py:501
  31.8 6.7 %collective-permute-start.18 = (bf16[1,272,128]{2,1,0:T(8,128)(2,1)S(1)}, bf16[1,272,128]{2,1,0:T(8,128)(2,1)S(1)}, u32[]{:S(2)}, u32[]{:S(2)}) collective-permute-start(bf16[1,272,128]{2,1,0:T(8,128)(2,1)S(1)} %get-tuple-element.44), channel_id=1, source_target_pairs={{0,24},{8,16},{16,8},{24,0},{1,25},{9,17},{17,9},{25,1},{2,26},{10... | collective-permute-start | bytes 208904 | tf_op jit(solution)/shard_map/ppermute | solution.py:501
  32.3 1.4 %collective-permute-start.10 = (bf16[128,512]{1,0:T(8,128)(2,1)S(1)}, bf16[128,512]{1,0:T(8,128)(2,1)S(1)}, u32[]{:S(2)}, u32[]{:S(2)}) collective-permute-start(bf16[128,512]{1,0:T(8,128)(2,1)S(1)} %collective-permute-done.9.refs_2_), channel_id=1, source_target_pairs={{0,1},{1,0},{2,3},{3,2},{4,5},{5,4},{6,7},{7,6},{8,9},{9,8},{10,11... | collective-permute-start | bytes 393224 | tf_op jit(solution)/shard_map/ppermute | solution.py:498
  32.3 1.5 %collective-permute-start.8 = (bf16[128,512]{1,0:T(8,128)(2,1)S(1)}, bf16[128,512]{1,0:T(8,128)(2,1)S(1)}, u32[]{:S(2)}, u32[]{:S(2)}) collective-permute-start(bf16[128,512]{1,0:T(8,128)(2,1)S(1)} %collective-permute-done.refs_0_), channel_id=1, source_target_pairs={{0,1},{1,0},{2,3},{3,2},{4,5},{5,4},{6,7},{7,6},{8,9},{9,8},{10,11... | collective-permute-start | bytes 393224 | tf_op jit(solution)/shard_map/ppermute | solution.py:498
  33.8 4.7 %copy-start.6 = (bf16[2,512]{1,0:T(2,128)(2,1)S(1)}, bf16[2,512]{1,0:T(2,128)(2,1)}, u32[]{:S(2)}) copy-start(bf16[2,512]{1,0:T(2,128)(2,1)} %refs_4_.7) | copy-start | bytes 6148
  33.8 4.7 %copy-start.7 = (bf16[2,512]{1,0:T(2,128)(2,1)S(1)}, bf16[2,512]{1,0:T(2,128)(2,1)}, u32[]{:S(2)}) copy-start(bf16[2,512]{1,0:T(2,128)(2,1)} %refs_5_.7) | copy-start | bytes 6148
  33.8 4.7 %copy-start.8 = (f32[2,4]{1,0:T(2,128)S(1)}, f32[2,4]{1,0:T(2,128)}, u32[]{:S(2)}) copy-start(f32[2,4]{1,0:T(2,128)} %refs_6_.7) | copy-start | bytes 100
  35.0 6.3 %collective-permute-start.13 = (bf16[1,272,128]{2,1,0:T(8,128)(2,1)S(1)}, bf16[1,272,128]{2,1,0:T(8,128)(2,1)S(1)}, u32[]{:S(2)}, u32[]{:S(2)}) collective-permute-start(bf16[1,272,128]{2,1,0:T(8,128)(2,1)S(1)} %get-tuple-element.51), channel_id=1, source_target_pairs={{0,8},{8,0},{16,24},{24,16},{1,9},{9,1},{17,25},{25,17},{2,10},{10... | collective-permute-start | bytes 208904 | tf_op jit(solution)/shard_map/ppermute | solution.py:501
  36.5 4.8 %collective-permute-start.14 = (bf16[1,272,128]{2,1,0:T(8,128)(2,1)S(1)}, bf16[1,272,128]{2,1,0:T(8,128)(2,1)S(1)}, u32[]{:S(2)}, u32[]{:S(2)}) collective-permute-start(bf16[1,272,128]{2,1,0:T(8,128)(2,1)S(1)} %get-tuple-element.52), channel_id=1, source_target_pairs={{0,16},{8,24},{16,0},{24,8},{1,17},{9,25},{17,1},{25,9},{2,18},{10... | collective-permute-start | bytes 208904 | tf_op jit(solution)/shard_map/ppermute | solution.py:501
  38.0 5.2 %collective-permute-start.15 = (bf16[1,272,128]{2,1,0:T(8,128)(2,1)S(1)}, bf16[1,272,128]{2,1,0:T(8,128)(2,1)S(1)}, u32[]{:S(2)}, u32[]{:S(2)}) collective-permute-start(bf16[1,272,128]{2,1,0:T(8,128)(2,1)S(1)} %get-tuple-element.53), channel_id=1, source_target_pairs={{0,24},{8,16},{16,8},{24,0},{1,25},{9,17},{17,9},{25,1},{2,26},{10... | collective-permute-start | bytes 208904 | tf_op jit(solution)/shard_map/ppermute | solution.py:501
  46.0 3.8 %collective-permute-start.19 = (bf16[2,1,48,128]{3,2,1,0:T(8,128)(2,1)S(1)}, bf16[2,1,48,128]{3,2,1,0:T(8,128)(2,1)S(1)}, u32[]{:S(2)}, u32[]{:S(2)}) collective-permute-start(bf16[2,1,48,128]{3,2,1,0:T(8,128)(2,1)S(1)} %get-tuple-element.59), channel_id=1, source_target_pairs={{0,8},{8,0},{16,24},{24,16},{1,9},{9,1},{17,25},{25,17},{2,10},{10... | collective-permute-start | bytes 73736 | tf_op jit(solution)/shard_map/ppermute | solution.py:501
  46.5 3.8 %collective-permute-start.20 = (bf16[2,1,48,128]{3,2,1,0:T(8,128)(2,1)S(1)}, bf16[2,1,48,128]{3,2,1,0:T(8,128)(2,1)S(1)}, u32[]{:S(2)}, u32[]{:S(2)}) collective-permute-start(bf16[2,1,48,128]{3,2,1,0:T(8,128)(2,1)S(1)} %get-tuple-element.60), channel_id=1, source_target_pairs={{0,16},{8,24},{16,0},{24,8},{1,17},{9,25},{17,1},{25,9},{2,18},{10... | collective-permute-start | bytes 73736 | tf_op jit(solution)/shard_map/ppermute | solution.py:501
  47.1 4.7 %collective-permute-start.21 = (bf16[2,1,48,128]{3,2,1,0:T(8,128)(2,1)S(1)}, bf16[2,1,48,128]{3,2,1,0:T(8,128)(2,1)S(1)}, u32[]{:S(2)}, u32[]{:S(2)}) collective-permute-start(bf16[2,1,48,128]{3,2,1,0:T(8,128)(2,1)S(1)} %get-tuple-element.61), channel_id=1, source_target_pairs={{0,24},{8,16},{16,8},{24,0},{1,25},{9,17},{17,9},{25,1},{2,26},{10... | collective-permute-start | bytes 73736 | tf_op jit(solution)/shard_map/ppermute | solution.py:501
where the time goes:
time: 52.7 us; the launch traced here: 52.5 us
  starting transfers between devices  27 us (51%)
  waiting for transfers between devices  11 us (21%)
  Pallas kernels  10.8 us (20%)
  local copies, waits for them, and re-layouts  3.01 us (6%)
  between operations  0.76 us (1%)
    ppermute x6, starting transfers between devices, over_tp(): return lax.ppermute(array, 'tp', links)  15 us
    pallas_call x8, Pallas kernels, kernel(): pl.pallas_call(body, out_shape=[jax.ShapeDtypeStruct(*shape) for shape in...  10.8 us
    ppermute x9, starting transfers between devices, over_sp(): return lax.ppermute(array, 'sp', [(i, i ^ step) for i in range(group)])  10.6 us
    ppermute x6, waiting for transfers between devices, over_tp(): return lax.ppermute(array, 'tp', links)  6.54 us
    ppermute x9, waiting for transfers between devices, over_sp(): return lax.ppermute(array, 'sp', [(i, i ^ step) for i in range(group)])  4.31 us
    unnamed x22, local copies, waits for them, and re-layouts  2.02 us
    ppermute x7, starting transfers between devices, to_partner(): return lax.ppermute(array, 'tp', [(i, i ^ 1) for i in range(members)])  1.33 us
  transfers between devices with their start and end apart: 22, of which 6 were waited for; matrix products, arithmetic and copies ran while one was open for 0% of the time, Pallas kernels for 14%

commit v1 on v0

--- a/solution.py
+++ b/solution.py
@@ -231,12 +231,16 @@
     gain_out[...] = placed(gain_ref[...])
 
 
-def partial_kernel(sources, s, *refs):
+def partial_kernel(sources, s, chained, *refs):
+    before, refs = (refs[:2], refs[2:]) if chained else ((), refs)
     pieces, (key_ref, value_ref, gate_ref) = refs[: len(sources)], refs[len(sources) : -2]
     total_ref, gates_ref = refs[-2:]
     positions = total_ref.shape[0]
     width = key_ref.shape[1]
     total_key = total_value = total_gate = 0.0
+    if chained:
+        total_key, total_value = before[0][:, :width], before[0][:, width:]
+        total_gate = before[1][...]
     for piece, (lane, step) in zip(pieces, sources):
         rows = source_rows(lane, step, piece.shape[1])
         block = piece[...] if step else piece[pl.ds(s * positions, positions), :]
@@ -361,27 +365,13 @@
     return powers(lefts, steps, 1, extent // small)
 
 
-def state_kernel(s, group, *refs):
-    blocks = refs[:group]
-    query_ref, new_key_ref, strengths = refs[group : group + 3]
-    earlier = refs[group + 3 : -group - 3]
-    outs = refs[-group - 3 : -3]
-    maps, adds, turned = refs[-3:]
-    for m in range(group if earlier else 0):
-        outs[m][:s] = earlier[m][...]
-    place = lax.axis_index("sp")
-    share = blocks[0].shape[0]
-    positions = (blocks[0].shape[1] - SIDE) // 2
-    width = blocks[0].shape[2]
+def block_maps(keys, values, sides):
+    count = len(keys)
+    positions = keys[0].shape[0]
     row_at = lax.broadcasted_iota(jnp.int32, (positions, positions), 0)
     col_at = lax.broadcasted_iota(jnp.int32, (positions, positions), 1)
     eye = row_at == col_at
-    units = [(r, m) for r in range(share) for m in range(group)]
-    count = len(units)
-    keys = [blocks[m][r, pl.ds(0, positions), :] for r, m in units]
     grams = [dot_nt(key, key) for key in keys]
-    values = [blocks[m][r, pl.ds(positions, positions), :] for r, m in units]
-    sides = [blocks[m][r, pl.ds(2 * positions, SIDE), :].astype(jnp.float32) for r, m in units]
     decays = [side[0:1] + side[1:2] + side[2:3] for side in sides]
     strength_rows = [side[3:4] + side[4:5] + side[5:6] for side in sides]
     lines = jnp.concatenate([*decays, jnp.zeros((-count % 8, positions), jnp.float32)], axis=0)
@@ -406,13 +396,55 @@
         for u in range(count)
     ]
     lefts = over_unit_lower(lefts, mixings, row_at, col_at)
-    for u, (r, m) in enumerate(units):
-        slot = r * group + (place ^ m)
-        adds[slot] = dot_left(lefts[u] * (squares[u] * scales[u]), values[u])
+    results = []
+    for u in range(count):
+        add = dot_left(lefts[u] * (squares[u] * scales[u]), values[u])
         erase = dot_left(lefts[u] * jnp.exp(decays[u]), keys[u])
-        maps[slot] = jnp.where(eye, jnp.exp(finals[u]), 0.0) - erase
+        read_map = jnp.where(eye, jnp.exp(finals[u]), 0.0) - erase
+        results.append(jnp.concatenate([read_map, add], axis=1))
+    return results
+
+
+def state_kernel(s, last, group, *refs):
+    refs = list(refs)
+    blocks = [refs.pop(0) for _ in range(group)]
+    query_ref, new_key_ref, strengths = (refs.pop(0) for _ in range(3))
+    earlier = [refs.pop(0) for _ in range(group)] if s else []
+    held = refs.pop(0) if s else None
+    following = None if last else refs.pop(0)
+    outs = [refs.pop(0) for _ in range(group)]
+    held_out = None if last else refs.pop(0)
+    maps, turned = refs
+    for before, out in zip(earlier, outs):
+        out[:s] = before[...]
+    place = lax.axis_index("sp")
+    share = blocks[0].shape[0]
+    positions = (blocks[0].shape[1] - SIDE) // 2
+    width = blocks[0].shape[2]
+
+    def taken(ref, r):
+        return (
+            ref[r, pl.ds(0, positions), :],
+            ref[r, pl.ds(positions, positions), :],
+            ref[r, pl.ds(2 * positions, SIDE), :].astype(jnp.float32),
+        )
+
+    units = [(r, m) for r in range(share) for m in range(group) if m or held is None]
+    sources = [taken(blocks[m], r) for r, m in units]
+    if following is not None:
+        sources += [taken(following, r) for r in range(share)]
+    results = block_maps(*zip(*sources))
+    for (r, m), result in zip(units, results):
+        maps[r * group + (place ^ m)] = result
     for r in range(share):
-        level = [(maps[r * group + b], adds[r * group + b]) for b in range(group)]
+        if held is not None:
+            maps[r * group + place] = held[r]
+        if following is not None:
+            held_out[r] = results[len(units) + r]
+    for r in range(share):
+        level = [
+            (maps[r * group + b, :, :width], maps[r * group + b, :, width:]) for b in range(group)
+        ]
         while len(level) > 1:
             joined = []
             for b in range(0, len(level), 2):
@@ -429,14 +461,18 @@
         query = query_ref[:, spot].astype(jnp.float32)[s : s + 1]
         new_key = new_key_ref[:, spot].astype(jnp.float32)[s : s + 1]
         unit_new = new_key * lax.rsqrt(jnp.sum(new_key * new_key, axis=-1, keepdims=True) + 1e-06)
-        both = jnp.concatenate([query, unit_new, jnp.zeros((6, width), jnp.float32)], axis=0)
+        both = jnp.concatenate([query, unit_new, jnp.zeros((6, width), jnp.float32)], axis=0).T
         overlap = jnp.sum(query * unit_new, axis=-1, keepdims=True)
         lane_at = lax.broadcasted_iota(jnp.int32, strengths.shape, 1)
         strength = jnp.sum(jnp.where(lane_at == head, strengths[...], 0.0), axis=1, keepdims=True)
-        fresh_row = sum(sides[r * group + m][6:7] for m in range(group))
-        gain_row = sum(sides[r * group + m][j : j + 1] for m in range(group) for j in (7, 8, 9))
-        reads = dot_wide(both, state)
-        raw = reads[0:1] + strength[s : s + 1] * overlap * (fresh_row - reads[1:2])
+        sides = [
+            block[r, pl.ds(2 * positions, SIDE), :].astype(jnp.float32) for block in blocks
+        ]
+        fresh_row = sum(side[6:7] for side in sides)
+        gain_row = sum(side[j : j + 1] for side in sides for j in (7, 8, 9))
+        query_read = jnp.sum(both[:, 0:1] * state, axis=0, keepdims=True)
+        key_read = jnp.sum(both[:, 1:2] * state, axis=0, keepdims=True)
+        raw = query_read + strength[s : s + 1] * overlap * (fresh_row - key_read)
         first = raw * lax.rsqrt(jnp.mean(raw * raw, axis=-1, keepdims=True) + 1e-06) * gain_row
         turned[...] = state.T.astype(jnp.bfloat16)
         tail = jnp.broadcast_to(first, (SIDE, first.shape[1])).astype(jnp.bfloat16)
@@ -543,16 +579,23 @@
             arrived += [piece, to_partner(piece)]
         early = len(arrived) - 4
         weights = [key_matrix, value_matrix, gate_matrix.T]
-        totals = kernel(
-            functools.partial(partial_kernel, [(0, 0), (1, 0), *pairs[:early]], s),
-            12,
-            PROJECT_FLOPS,
-            [((positions, 2 * wide), f32), ((gate_matrix.shape[1], positions), f32)],
-            [],
-            [own, partner, *arrived[:early], *weights],
-        )
+        late = list(range(early, len(arrived)))
+        stages = [([(0, 0), (1, 0), *pairs[:early]], [own, partner, *arrived[:early]])]
+        if s:
+            here, late = late[::2], late[1::2]
+            stages.append(([pairs[n] for n in here], [arrived[n] for n in here]))
+        totals = []
+        for n, (sources, pieces) in enumerate(stages):
+            totals = kernel(
+                functools.partial(partial_kernel, sources, s, n > 0),
+                12,
+                PROJECT_FLOPS,
+                [((positions, 2 * wide), f32), ((gate_matrix.shape[1], positions), f32)],
+                [],
+                [*totals, *pieces, *weights],
+            )
         messages = kernel(
-            functools.partial(project_kernel, pairs[early:], s, group),
+            functools.partial(project_kernel, [pairs[n] for n in late], s, group),
             12,
             PROJECT_FLOPS,
             [((share, rows, width), bf16)] * group,
@@ -564,7 +607,7 @@
                 pltpu.VMEM((heads, positions), f32),
             ],
             [
-                *arrived[early:],
+                *(arrived[n] for n in late),
                 *totals,
                 *weights,
                 extra_log_decay,
@@ -573,20 +616,30 @@
         )
         after = tuple(messages)
         blocks.append([messages[0]] + [over_sp(messages[m], m) for m in range(1, group)])
-    results = []
+    results, held = [], []
     for s in range(sequences):
+        last = s + 1 == sequences
+        map_shape = ((share, width, width + value_width), f32)
         results = kernel(
-            functools.partial(state_kernel, s, group),
+            functools.partial(state_kernel, s, last, group),
             8,
             STATE_FLOPS,
-            [((s + 1, share, out_rows, width), bf16)] * group,
+            [((s + 1, share, out_rows, width), bf16)] * group + ([] if last else [map_shape]),
             [
-                pltpu.VMEM((heads, width, value_width), f32),
-                pltpu.VMEM((heads, width, width), f32),
+                pltpu.VMEM((heads, width, width + value_width), f32),
                 pltpu.VMEM((value_width, width), bf16),
             ],
-            [*blocks[s], next_token_query, next_token_key, next_write_strength, *results],
-        )
+            [
+                *blocks[s],
+                next_token_query,
+                next_token_key,
+                next_write_strength,
+                *results,
+                *held,
+                *([] if last else [blocks[s + 1][0]]),
+            ],
+        )
+        held, results = results[group:], results[:group]
     parts = [results[0]] + [over_sp(results[m], m) for m in range(1, group)]
     turned_state, first_read = kernel(
         functools.partial(finish_kernel, group),

time: 52.7 us -> 52.8 us (level)
    pallas_call x8 -> x9, Pallas kernels: 10.8 us -> 10.9 us  [kernel(): pl.pallas_call(body, out_shape=[jax.ShapeDtypeStruct(*shape) for shape in...]
  transfers between devices with their start and end apart: 22 -> 22, of which waited for: 6 -> 5; matrix products, arithmetic and copies ran while one was open for 0% -> 0% of each run, Pallas kernels for 14% -> 15%
where the time goes in v1:
time: 52.8 us; the launch traced here: 52.6 us
  starting transfers between devices  27 us (51%)
  Pallas kernels  10.9 us (21%)
  waiting for transfers between devices  10.8 us (20%)
  local copies, waits for them, and re-layouts  3.02 us (6%)
  between operations  0.81 us (2%)
    ppermute x6, starting transfers between devices, over_tp(): return lax.ppermute(array, 'tp', links)  15 us
    pallas_call x9, Pallas kernels, kernel(): pl.pallas_call(body, out_shape=[jax.ShapeDtypeStruct(*shape) for shape in...  10.9 us
    ppermute x9, starting transfers between devices, over_sp(): return lax.ppermute(array, 'sp', [(i, i ^ step) for i in range(group)])  10.7 us
    ppermute x6, waiting for transfers between devices, over_tp(): return lax.ppermute(array, 'tp', links)  6.54 us
    ppermute x9, waiting for transfers between devices, over_sp(): return lax.ppermute(array, 'sp', [(i, i ^ step) for i in range(group)])  4.26 us
    unnamed x22, local copies, waits for them, and re-layouts  2.03 us
    ppermute x7, starting transfers between devices, to_partner(): return lax.ppermute(array, 'tp', [(i, i ^ 1) for i in range(members)])  1.33 us
  transfers between devices with their start and end apart: 22, of which 5 were waited for; matrix products, arithmetic and copies ran while one was open for 0% of the time, Pallas kernels for 15%

profile of v1, /device:TPU:0, one launch (start us, length us, event | category | flops | bytes accessed | tf_op | source)
XLA Modules:
  0.0 52.6 jit_solution(8642827811684890632)
XLA Ops:
  0.6 1.0 %slice_bitcast_fusion = (bf16[128,512]{1,0:T(8,128)(2,1)S(1)}, bf16[128,512]{1,0:T(8,128)(2,1)S(1)}) fusion(bf16[2,128,512]{2,1,0:T(8,128)(2,1)} %param.11), kind=kLoop, calls=%fused_computation | loop fusion | bytes 524288 | tf_op jit(solution)/shard_map/squeeze | solution.py:558
  1.6 3.1 %collective-permute-start.6 = (bf16[128,512]{1,0:T(8,128)(2,1)S(1)}, bf16[128,512]{1,0:T(8,128)(2,1)S(1)}, u32[]{:S(2)}, u32[]{:S(2)}) collective-permute-start(bf16[128,512]{1,0:T(8,128)(2,1)S(1)} %get-tuple-element.70), channel_id=1, source_target_pairs={{0,2},{1,3},{2,0},{3,1},{4,6},{5,7},{6,4},{7,5},{8,10},{9,11},{10,... | collective-permute-start | bytes 393224 | tf_op jit(solution)/shard_map/ppermute | solution.py:531
  4.7 2.6 %collective-permute-start.1 = (bf16[128,512]{1,0:T(8,128)(2,1)S(1)}, bf16[128,512]{1,0:T(8,128)(2,1)S(1)}, u32[]{:S(2)}, u32[]{:S(2)}) collective-permute-start(bf16[128,512]{1,0:T(8,128)(2,1)S(1)} %get-tuple-element.70), channel_id=1, source_target_pairs={{0,4},{1,5},{2,6},{3,7},{4,0},{5,1},{6,2},{7,3},{8,12},{9,13},{10,... | collective-permute-start | bytes 393224 | tf_op jit(solution)/shard_map/ppermute | solution.py:531
  7.3 0.0 collective-permute-start.3
  7.3 0.0 collective-permute-start.5
  7.3 0.9 %collective-permute-start.11 = (bf16[128,512]{1,0:T(8,128)(2,1)S(1)}, bf16[128,512]{1,0:T(8,128)(2,1)S(1)}, u32[]{:S(2)}, u32[]{:S(2)}) collective-permute-start(bf16[128,512]{1,0:T(8,128)(2,1)S(1)} %get-tuple-element.71), channel_id=1, source_target_pairs={{0,2},{1,3},{2,0},{3,1},{4,6},{5,7},{6,4},{7,5},{8,10},{9,11},{10,... | collective-permute-start | bytes 393224 | tf_op jit(solution)/shard_map/ppermute | solution.py:531
  8.2 0.7 %copy-done.5 = bf16[2,4,32]{2,1,0:T(4,128)(2,1)S(1)} copy-done((bf16[2,4,32]{2,1,0:T(4,128)(2,1)S(1)}, bf16[2,4,32]{2,1,0:T(4,128)(2,1)}, u32[]{:S(2)}) %copy-start.5) | copy-done | bytes 536
  8.9 0.7 %copy-done.9 = f32[4]{0:T(128)S(1)} copy-done((f32[4]{0:T(128)S(1)}, f32[4]{0:T(128)}, u32[]{:S(2)}) %copy-start.9) | copy-done | bytes 40
  9.6 0.7 %copy-done.10 = f32[32]{0:T(128)S(1)} copy-done((f32[32]{0:T(128)S(1)}, f32[32]{0:T(128)}, u32[]{:S(2)}) %copy-start.10) | copy-done | bytes 152
  10.2 0.6 %shard_map.122 = (f32[4,128]{1,0:T(4,128)S(1)}, f32[2,4,128]{2,1,0:T(4,128)S(1)}, f32[1,128]{1,0:T(1,128)S(1)}) custom-call(f32[4]{0:T(128)S(1)} %copy-done.9, bf16[2,4,32]{2,1,0:T(4,128)(2,1)S(1)} %copy-done.5, f32[1,32]{1,0:T(1,128)S(1)} %bitcast.16), custom_call_target="tpu_custom_call" | custom-call | flops 4000000000 | tf_op jit(solution)/shard_map/pallas_call | solution.py:543
  10.9 0.0 collective-permute-done.6.refs_2_
  10.9 0.2 collective-permute-start.7
  11.1 6.5 %collective-permute-done.1.refs_0_ = bf16[128,512]{1,0:T(8,128)(2,1)S(1)} collective-permute-done((bf16[128,512]{1,0:T(8,128)(2,1)S(1)}, bf16[128,512]{1,0:T(8,128)(2,1)S(1)}, u32[]{:S(2)}, u32[]{:S(2)}) %collective-permute-start.1) | collective-permute-done | bytes 131104 | tf_op jit(solution)/shard_map/ppermute | solution.py:531
  17.6 2.3 %collective-permute-start.9 = (bf16[128,512]{1,0:T(8,128)(2,1)S(1)}, bf16[128,512]{1,0:T(8,128)(2,1)S(1)}, u32[]{:S(2)}, u32[]{:S(2)}) collective-permute-start(bf16[128,512]{1,0:T(8,128)(2,1)S(1)} %get-tuple-element.71), channel_id=1, source_target_pairs={{0,6},{1,7},{2,4},{3,5},{4,2},{5,3},{6,0},{7,1},{8,14},{9,15},{10,... | collective-permute-start | bytes 393224 | tf_op jit(solution)/shard_map/ppermute | solution.py:531
  19.9 6.1 %collective-permute-start = (bf16[128,512]{1,0:T(8,128)(2,1)S(1)}, bf16[128,512]{1,0:T(8,128)(2,1)S(1)}, u32[]{:S(2)}, u32[]{:S(2)}) collective-permute-start(bf16[128,512]{1,0:T(8,128)(2,1)S(1)} %get-tuple-element.71), channel_id=1, source_target_pairs={{0,4},{1,5},{2,6},{3,7},{4,0},{5,1},{6,2},{7,3},{8,12},{9,13},{10,... | collective-permute-start | bytes 393224 | tf_op jit(solution)/shard_map/ppermute | solution.py:531
  26.1 0.0 collective-permute-done.11.refs_2_
  26.1 0.0 collective-permute-start.2
  26.1 0.0 collective-permute-done.7.refs_3_
  26.1 0.5 collective-permute-start.4
  26.6 0.0 collective-permute-done.5.refs_1_
  26.6 0.1 collective-permute-start.12
  26.7 0.0 copy-start.4
  26.7 0.9 %shard_map.123 = (f32[128,1024]{1,0:T(8,128)S(1)}, f32[64,128]{1,0:T(8,128)S(1)}) custom-call(bf16[256,512]{1,0:T(8,128)(2,1)S(1)} %bitcast.14, bf16[256,512]{1,0:T(8,128)(2,1)S(1)} %collective-permute-done.5.refs_1_, bf16[128,512]{1,0:T(8,128)(2,1)S(1)} %collective-permute-done.6.refs_2_, bf16[128,512]{1,0:T(8,128)(2,1)S(1)} %collective-permute-done.7.refs_3_, ...), custom_call_target="tpu_custom_call" | custom-call | flops 2000000000 | tf_op jit(solution)/shard_map/pallas_call | solution.py:543
  27.6 0.0 collective-permute-done.4.refs_3_
  27.6 1.1 %shard_map.124 = (bf16[1,272,128]{2,1,0:T(8,128)(2,1)S(1)}, bf16[1,272,128]{2,1,0:T(8,128)(2,1)S(1)}, bf16[1,272,128]{2,1,0:T(8,128)(2,1)S(1)}, bf16[1,272,128]{2,1,0:T(8,128)(2,1)S(1)}) custom-call(bf16[128,512]{1,0:T(8,128)(2,1)S(1)} %collective-permute-done.1.refs_0_, bf16[128,512]{1,0:T(8,128)(2,1)S(1)} %collective-permute-done.2.refs_1_, ...), custom_call_target="tpu_custom_call" | custom-call | flops 2000000000 | tf_op jit(solution)/shard_map/pallas_call | solution.py:543
  28.7 1.6 %collective-permute-start.16 = (bf16[1,272,128]{2,1,0:T(8,128)(2,1)S(1)}, bf16[1,272,128]{2,1,0:T(8,128)(2,1)S(1)}, u32[]{:S(2)}, u32[]{:S(2)}) collective-permute-start(bf16[1,272,128]{2,1,0:T(8,128)(2,1)S(1)} %get-tuple-element.45), channel_id=1, source_target_pairs={{0,8},{8,0},{16,24},{24,16},{1,9},{9,1},{17,25},{25,17},{2,10},{10... | collective-permute-start | bytes 208904 | tf_op jit(solution)/shard_map/ppermute | solution.py:537
  30.3 1.5 %collective-permute-start.17 = (bf16[1,272,128]{2,1,0:T(8,128)(2,1)S(1)}, bf16[1,272,128]{2,1,0:T(8,128)(2,1)S(1)}, u32[]{:S(2)}, u32[]{:S(2)}) collective-permute-start(bf16[1,272,128]{2,1,0:T(8,128)(2,1)S(1)} %get-tuple-element.46), channel_id=1, source_target_pairs={{0,16},{8,24},{16,0},{24,8},{1,17},{9,25},{17,1},{25,9},{2,18},{10... | collective-permute-start | bytes 208904 | tf_op jit(solution)/shard_map/ppermute | solution.py:537
  31.8 0.5 collective-permute-start.18
  32.3 0.5 collective-permute-start.8
  32.8 0.9 %shard_map.125 = (f32[128,1024]{1,0:T(8,128)S(1)}, f32[64,128]{1,0:T(8,128)S(1)}) custom-call(bf16[256,512]{1,0:T(8,128)(2,1)S(1)} %bitcast.15, bf16[256,512]{1,0:T(8,128)(2,1)S(1)} %collective-permute-done.5.refs_1_, bf16[128,512]{1,0:T(8,128)(2,1)S(1)} %collective-permute-done.11.refs_2_, bf16[128,512]{1,0:T(8,128)(2,1)S(1)} %collective-permute-done.12.refs_3_, ...), custom_call_target="tpu_custom_call" | custom-call | flops 2000000000 | tf_op jit(solution)/shard_map/pallas_call | solution.py:543
  33.7 0.5 %shard_map.126 = (f32[128,1024]{1,0:T(8,128)S(1)}, f32[64,128]{1,0:T(8,128)S(1)}) custom-call(f32[128,1024]{1,0:T(8,128)S(1)} %get-tuple-element.51.refs_0_, f32[64,128]{1,0:T(8,128)S(1)} %get-tuple-element.52.refs_1_, bf16[128,512]{1,0:T(8,128)(2,1)S(1)} %collective-permute-done.refs_2_, bf16[128,512]{1,0:T(8,128)(2,1)S(1)} %collective-permute-done.9.refs_3_, ...), custom_call_target="tpu_custom_call" | custom-call | flops 2000000000 | tf_op jit(solution)/shard_map/pallas_call | solution.py:543
  34.3 0.0 copy-start.6
  34.3 0.0 copy-start.7
  34.3 0.0 copy-start.8
  34.3 0.8 %shard_map.127 = (bf16[1,272,128]{2,1,0:T(8,128)(2,1)S(1)}, bf16[1,272,128]{2,1,0:T(8,128)(2,1)S(1)}, bf16[1,272,128]{2,1,0:T(8,128)(2,1)S(1)}, bf16[1,272,128]{2,1,0:T(8,128)(2,1)S(1)}) custom-call(bf16[128,512]{1,0:T(8,128)(2,1)S(1)} %collective-permute-done.8.refs_0_, bf16[128,512]{1,0:T(8,128)(2,1)S(1)} %collective-permute-done.10.refs_1_, ...), custom_call_target="tpu_custom_call" | custom-call | flops 2000000000 | tf_op jit(solution)/shard_map/pallas_call | solution.py:543
  35.1 1.6 %collective-permute-start.13 = (bf16[1,272,128]{2,1,0:T(8,128)(2,1)S(1)}, bf16[1,272,128]{2,1,0:T(8,128)(2,1)S(1)}, u32[]{:S(2)}, u32[]{:S(2)}) collective-permute-start(bf16[1,272,128]{2,1,0:T(8,128)(2,1)S(1)} %get-tuple-element.56), channel_id=1, source_target_pairs={{0,8},{8,0},{16,24},{24,16},{1,9},{9,1},{17,25},{25,17},{2,10},{10... | collective-permute-start | bytes 208904 | tf_op jit(solution)/shard_map/ppermute | solution.py:537
  36.6 1.5 %collective-permute-start.14 = (bf16[1,272,128]{2,1,0:T(8,128)(2,1)S(1)}, bf16[1,272,128]{2,1,0:T(8,128)(2,1)S(1)}, u32[]{:S(2)}, u32[]{:S(2)}) collective-permute-start(bf16[1,272,128]{2,1,0:T(8,128)(2,1)S(1)} %get-tuple-element.57), channel_id=1, source_target_pairs={{0,16},{8,24},{16,0},{24,8},{1,17},{9,25},{17,1},{25,9},{2,18},{10... | collective-permute-start | bytes 208904 | tf_op jit(solution)/shard_map/ppermute | solution.py:537
  38.1 0.5 collective-permute-start.15
  38.7 2.8 %shard_map.128 = (bf16[1,1,48,128]{3,2,1,0:T(8,128)(2,1)S(1)}, bf16[1,1,48,128]{3,2,1,0:T(8,128)(2,1)S(1)}, bf16[1,1,48,128]{3,2,1,0:T(8,128)(2,1)S(1)}, bf16[1,...) custom-call(bf16[1,272,128]{2,1,0:T(8,128)(2,1)S(1)} %get-tuple-element.44.refs_0_, ...), custom_call_target="tpu_custom_call" | custom-call | flops 4000000000 | tf_op jit(solution)/shard_map/pallas_call | solution.py:543
  41.5 1.8 %collective-permute-done.15.refs_3_ = bf16[1,272,128]{2,1,0:T(8,128)(2,1)S(1)} collective-permute-done((bf16[1,272,128]{2,1,0:T(8,128)(2,1)S(1)}, bf16[1,272,128]{2,1,0:T(8,128)(2,1)S(1)}, u32[]{:S(2)}, u32[]{:S(2)}) %collective-permute-start.15) | collective-permute-done | bytes 69664 | tf_op jit(solution)/shard_map/ppermute | solution.py:537
  43.3 2.6 %shard_map.129 = (bf16[2,1,48,128]{3,2,1,0:T(8,128)(2,1)S(1)}, bf16[2,1,48,128]{3,2,1,0:T(8,128)(2,1)S(1)}, bf16[2,1,48,128]{3,2,1,0:T(8,128)(2,1)S(1)}, bf16[2,1,48,128]{3,2,1,0:T(8,128)(2,1)S(1)}) custom-call(bf16[1,272,128]{2,1,0:T(8,128)(2,1)S(1)} %get-tuple-element.55.refs_7_.refs_0_, bf16[1,272,128]{2,1,0:T(8,128)(2,1)S(1)} %collective-permute-done.13.refs_1_, ...), custom_call_target="tpu_custom_call" | custom-call | flops 4000000000 | tf_op jit(solution)/shard_map/pallas_call | solution.py:543
  46.0 0.6 %collective-permute-start.19 = (bf16[2,1,48,128]{3,2,1,0:T(8,128)(2,1)S(1)}, bf16[2,1,48,128]{3,2,1,0:T(8,128)(2,1)S(1)}, u32[]{:S(2)}, u32[]{:S(2)}) collective-permute-start(bf16[2,1,48,128]{3,2,1,0:T(8,128)(2,1)S(1)} %get-tuple-element.65), channel_id=1, source_target_pairs={{0,8},{8,0},{16,24},{24,16},{1,9},{9,1},{17,25},{25,17},{2,10},{10... | collective-permute-start | bytes 73736 | tf_op jit(solution)/shard_map/ppermute | solution.py:537
  46.6 0.6 %collective-permute-start.20 = (bf16[2,1,48,128]{3,2,1,0:T(8,128)(2,1)S(1)}, bf16[2,1,48,128]{3,2,1,0:T(8,128)(2,1)S(1)}, u32[]{:S(2)}, u32[]{:S(2)}) collective-permute-start(bf16[2,1,48,128]{3,2,1,0:T(8,128)(2,1)S(1)} %get-tuple-element.66), channel_id=1, source_target_pairs={{0,16},{8,24},{16,0},{24,8},{1,17},{9,25},{17,1},{25,9},{2,18},{10... | collective-permute-start | bytes 73736 | tf_op jit(solution)/shard_map/ppermute | solution.py:537
  47.2 2.3 %collective-permute-start.21 = (bf16[2,1,48,128]{3,2,1,0:T(8,128)(2,1)S(1)}, bf16[2,1,48,128]{3,2,1,0:T(8,128)(2,1)S(1)}, u32[]{:S(2)}, u32[]{:S(2)}) collective-permute-start(bf16[2,1,48,128]{3,2,1,0:T(8,128)(2,1)S(1)} %get-tuple-element.67), channel_id=1, source_target_pairs={{0,24},{8,16},{16,8},{24,0},{1,25},{9,17},{17,9},{25,1},{2,26},{10... | collective-permute-start | bytes 73736 | tf_op jit(solution)/shard_map/ppermute | solution.py:537
  49.5 0.3 collective-permute-done.19.refs_1_
  49.9 0.5 %collective-permute-done.20.refs_2_ = bf16[2,1,48,128]{3,2,1,0:T(8,128)(2,1)S(1)} collective-permute-done((bf16[2,1,48,128]{3,2,1,0:T(8,128)(2,1)S(1)}, bf16[2,1,48,128]{3,2,1,0:T(8,128)(2,1)S(1)}, u32[]{:S(2)}, u32[]{:S(2)}) %collective-permute-start.20) | collective-permute-done | bytes 24608 | tf_op jit(solution)/shard_map/ppermute | solution.py:537
  50.4 1.5 %collective-permute-done.21.refs_3_ = bf16[2,1,48,128]{3,2,1,0:T(8,128)(2,1)S(1)} collective-permute-done((bf16[2,1,48,128]{3,2,1,0:T(8,128)(2,1)S(1)}, bf16[2,1,48,128]{3,2,1,0:T(8,128)(2,1)S(1)}, u32[]{:S(2)}, u32[]{:S(2)}) %collective-permute-start.21) | collective-permute-done | bytes 24608 | tf_op jit(solution)/shard_map/ppermute | solution.py:537
  51.9 0.7 %shard_map.130 = (bf16[2,4,32,128]{3,2,1,0:T(8,128)(2,1)}, bf16[2,4,32]{2,1,0:T(4,128)(2,1)}) custom-call(bf16[2,1,48,128]{3,2,1,0:T(8,128)(2,1)S(1)} %get-tuple-element.64.refs_0_, bf16[2,1,48,128]{3,2,1,0:T(8,128)(2,1)S(1)} %collective-permute-done.19.refs_1_, bf16[2,1,48,128]{3,2,1,0:T(8,128)(2,1)S(1)} %collective-permute-done.20.refs_2_, ...), custom_call_target="tpu_custom_call" | custom-call | flops 1000000 | tf_op jit(solution)/shard_map/pallas_call | solution.py:543
  (28 shorter events, 0.1 us)
Async XLA Ops:
  1.6 9.2 %collective-permute-start.6 = (bf16[128,512]{1,0:T(8,128)(2,1)S(1)}, bf16[128,512]{1,0:T(8,128)(2,1)S(1)}, u32[]{:S(2)}, u32[]{:S(2)}) collective-permute-start(bf16[128,512]{1,0:T(8,128)(2,1)S(1)} %get-tuple-element.70), channel_id=1, source_target_pairs={{0,2},{1,3},{2,0},{3,1},{4,6},{5,7},{6,4},{7,5},{8,10},{9,11},{10,... | collective-permute-start | bytes 393224 | tf_op jit(solution)/shard_map/ppermute | solution.py:531
  4.7 12.9 %collective-permute-start.1 = (bf16[128,512]{1,0:T(8,128)(2,1)S(1)}, bf16[128,512]{1,0:T(8,128)(2,1)S(1)}, u32[]{:S(2)}, u32[]{:S(2)}) collective-permute-start(bf16[128,512]{1,0:T(8,128)(2,1)S(1)} %get-tuple-element.70), channel_id=1, source_target_pairs={{0,4},{1,5},{2,6},{3,7},{4,0},{5,1},{6,2},{7,3},{8,12},{9,13},{10,... | collective-permute-start | bytes 393224 | tf_op jit(solution)/shard_map/ppermute | solution.py:531
  7.3 12.6 %collective-permute-start.3 = (bf16[128,512]{1,0:T(8,128)(2,1)S(1)}, bf16[128,512]{1,0:T(8,128)(2,1)S(1)}, u32[]{:S(2)}, u32[]{:S(2)}) collective-permute-start(bf16[128,512]{1,0:T(8,128)(2,1)S(1)} %get-tuple-element.70), channel_id=1, source_target_pairs={{0,6},{1,7},{2,4},{3,5},{4,2},{5,3},{6,0},{7,1},{8,14},{9,15},{10,... | collective-permute-start | bytes 393224 | tf_op jit(solution)/shard_map/ppermute | solution.py:531
  7.3 19.3 %collective-permute-start.5 = (bf16[256,512]{1,0:T(8,128)(2,1)}, bf16[256,512]{1,0:T(8,128)(2,1)S(1)}, u32[]{:S(2)}, u32[]{:S(2)}) collective-permute-start(bf16[256,512]{1,0:T(8,128)(2,1)} %bitcast.13), channel_id=1, source_target_pairs={{0,1},{1,0},{2,3},{3,2},{4,5},{5,4},{6,7},{7,6},{8,9},{9,8},{10,11... | collective-permute-start | bytes 786440 | tf_op jit(solution)/shard_map/ppermute | solution.py:534
  7.3 18.7 %collective-permute-start.11 = (bf16[128,512]{1,0:T(8,128)(2,1)S(1)}, bf16[128,512]{1,0:T(8,128)(2,1)S(1)}, u32[]{:S(2)}, u32[]{:S(2)}) collective-permute-start(bf16[128,512]{1,0:T(8,128)(2,1)S(1)} %get-tuple-element.71), channel_id=1, source_target_pairs={{0,2},{1,3},{2,0},{3,1},{4,6},{5,7},{6,4},{7,5},{8,10},{9,11},{10,... | collective-permute-start | bytes 393224 | tf_op jit(solution)/shard_map/ppermute | solution.py:531
  8.2 0.7 %copy-start.5 = (bf16[2,4,32]{2,1,0:T(4,128)(2,1)S(1)}, bf16[2,4,32]{2,1,0:T(4,128)(2,1)}, u32[]{:S(2)}) copy-start(bf16[2,4,32]{2,1,0:T(4,128)(2,1)} %value_ref.1) | copy-start | bytes 1540
  8.9 0.7 %copy-start.9 = (f32[4]{0:T(128)S(1)}, f32[4]{0:T(128)}, u32[]{:S(2)}) copy-start(f32[4]{0:T(128)} %rate_ref.1) | copy-start | bytes 52
  9.6 0.7 %copy-start.10 = (f32[32]{0:T(128)S(1)}, f32[32]{0:T(128)}, u32[]{:S(2)}) copy-start(f32[32]{0:T(128)} %param.21) | copy-start | bytes 388
  10.2 16.4 %copy-start = (bf16[4096,512]{1,0:T(8,128)(2,1)S(1)}, bf16[4096,512]{1,0:T(8,128)(2,1)}, u32[]{:S(2)}) copy-start(bf16[4096,512]{1,0:T(8,128)(2,1)} %refs_4_.9) | copy-start | bytes 12582916
  10.2 16.4 %copy-start.1 = (bf16[4096,512]{1,0:T(8,128)(2,1)S(1)}, bf16[4096,512]{1,0:T(8,128)(2,1)}, u32[]{:S(2)}) copy-start(bf16[4096,512]{1,0:T(8,128)(2,1)} %refs_5_.9) | copy-start | bytes 12582916
  10.2 16.4 %copy-start.2 = (bf16[4096,64]{0,1:T(8,128)(2,1)S(1)}, bf16[4096,64]{0,1:T(8,128)(2,1)}, u32[]{:S(2)}) copy-start(bf16[4096,64]{0,1:T(8,128)(2,1)} %param.14) | copy-start | bytes 1572868
  10.2 16.4 %copy-start.3 = (bf16[2,128,512]{2,1,0:T(8,128)(2,1)S(1)}, bf16[2,128,512]{2,1,0:T(8,128)(2,1)}, u32[]{:S(2)}) copy-start(bf16[2,128,512]{2,1,0:T(8,128)(2,1)} %param.11) | copy-start | bytes 786436
  10.9 15.2 %collective-permute-start.7 = (bf16[128,512]{1,0:T(8,128)(2,1)S(1)}, bf16[128,512]{1,0:T(8,128)(2,1)S(1)}, u32[]{:S(2)}, u32[]{:S(2)}) collective-permute-start(bf16[128,512]{1,0:T(8,128)(2,1)S(1)} %collective-permute-done.6.refs_2_), channel_id=1, source_target_pairs={{0,1},{1,0},{2,3},{3,2},{4,5},{5,4},{6,7},{7,6},{8,9},{9,8},{10,11... | collective-permute-start | bytes 393224 | tf_op jit(solution)/shard_map/ppermute | solution.py:534
  17.6 14.2 %collective-permute-start.9 = (bf16[128,512]{1,0:T(8,128)(2,1)S(1)}, bf16[128,512]{1,0:T(8,128)(2,1)S(1)}, u32[]{:S(2)}, u32[]{:S(2)}) collective-permute-start(bf16[128,512]{1,0:T(8,128)(2,1)S(1)} %get-tuple-element.71), channel_id=1, source_target_pairs={{0,6},{1,7},{2,4},{3,5},{4,2},{5,3},{6,0},{7,1},{8,14},{9,15},{10,... | collective-permute-start | bytes 393224 | tf_op jit(solution)/shard_map/ppermute | solution.py:531
  19.9 12.4 %collective-permute-start = (bf16[128,512]{1,0:T(8,128)(2,1)S(1)}, bf16[128,512]{1,0:T(8,128)(2,1)S(1)}, u32[]{:S(2)}, u32[]{:S(2)}) collective-permute-start(bf16[128,512]{1,0:T(8,128)(2,1)S(1)} %get-tuple-element.71), channel_id=1, source_target_pairs={{0,4},{1,5},{2,6},{3,7},{4,0},{5,1},{6,2},{7,3},{8,12},{9,13},{10,... | collective-permute-start | bytes 393224 | tf_op jit(solution)/shard_map/ppermute | solution.py:531
  26.1 1.5 %collective-permute-start.2 = (bf16[128,512]{1,0:T(8,128)(2,1)S(1)}, bf16[128,512]{1,0:T(8,128)(2,1)S(1)}, u32[]{:S(2)}, u32[]{:S(2)}) collective-permute-start(bf16[128,512]{1,0:T(8,128)(2,1)S(1)} %collective-permute-done.1.refs_0_), channel_id=1, source_target_pairs={{0,1},{1,0},{2,3},{3,2},{4,5},{5,4},{6,7},{7,6},{8,9},{9,8},{10,11... | collective-permute-start | bytes 393224 | tf_op jit(solution)/shard_map/ppermute | solution.py:534
  26.1 1.5 %collective-permute-start.4 = (bf16[128,512]{1,0:T(8,128)(2,1)S(1)}, bf16[128,512]{1,0:T(8,128)(2,1)S(1)}, u32[]{:S(2)}, u32[]{:S(2)}) collective-permute-start(bf16[128,512]{1,0:T(8,128)(2,1)S(1)} %collective-permute-done.3.refs_2_), channel_id=1, source_target_pairs={{0,1},{1,0},{2,3},{3,2},{4,5},{5,4},{6,7},{7,6},{8,9},{9,8},{10,11... | collective-permute-start | bytes 393224 | tf_op jit(solution)/shard_map/ppermute | solution.py:534
  26.6 5.7 %collective-permute-start.12 = (bf16[128,512]{1,0:T(8,128)(2,1)S(1)}, bf16[128,512]{1,0:T(8,128)(2,1)S(1)}, u32[]{:S(2)}, u32[]{:S(2)}) collective-permute-start(bf16[128,512]{1,0:T(8,128)(2,1)S(1)} %collective-permute-done.11.refs_2_), channel_id=1, source_target_pairs={{0,1},{1,0},{2,3},{3,2},{4,5},{5,4},{6,7},{7,6},{8,9},{9,8},{10,11... | collective-permute-start | bytes 393224 | tf_op jit(solution)/shard_map/ppermute | solution.py:534
  26.7 0.9 %copy-start.4 = (f32[2,4,128]{2,1,0:T(4,128)S(1)}, f32[2,4,128]{2,1,0:T(4,128)}, u32[]{:S(2)}) copy-start(f32[2,4,128]{2,1,0:T(4,128)} %refs_7_.3) | copy-start | bytes 12292
  28.7 9.4 %collective-permute-start.16 = (bf16[1,272,128]{2,1,0:T(8,128)(2,1)S(1)}, bf16[1,272,128]{2,1,0:T(8,128)(2,1)S(1)}, u32[]{:S(2)}, u32[]{:S(2)}) collective-permute-start(bf16[1,272,128]{2,1,0:T(8,128)(2,1)S(1)} %get-tuple-element.45), channel_id=1, source_target_pairs={{0,8},{8,0},{16,24},{24,16},{1,9},{9,1},{17,25},{25,17},{2,10},{10... | collective-permute-start | bytes 208904 | tf_op jit(solution)/shard_map/ppermute | solution.py:537
  30.3 8.3 %collective-permute-start.17 = (bf16[1,272,128]{2,1,0:T(8,128)(2,1)S(1)}, bf16[1,272,128]{2,1,0:T(8,128)(2,1)S(1)}, u32[]{:S(2)}, u32[]{:S(2)}) collective-permute-start(bf16[1,272,128]{2,1,0:T(8,128)(2,1)S(1)} %get-tuple-element.46), channel_id=1, source_target_pairs={{0,16},{8,24},{16,0},{24,8},{1,17},{9,25},{17,1},{25,9},{2,18},{10... | collective-permute-start | bytes 208904 | tf_op jit(solution)/shard_map/ppermute | solution.py:537
  31.8 6.8 %collective-permute-start.18 = (bf16[1,272,128]{2,1,0:T(8,128)(2,1)S(1)}, bf16[1,272,128]{2,1,0:T(8,128)(2,1)S(1)}, u32[]{:S(2)}, u32[]{:S(2)}) collective-permute-start(bf16[1,272,128]{2,1,0:T(8,128)(2,1)S(1)} %get-tuple-element.47), channel_id=1, source_target_pairs={{0,24},{8,16},{16,8},{24,0},{1,25},{9,17},{17,9},{25,1},{2,26},{10... | collective-permute-start | bytes 208904 | tf_op jit(solution)/shard_map/ppermute | solution.py:537
  32.3 1.9 %collective-permute-start.10 = (bf16[128,512]{1,0:T(8,128)(2,1)S(1)}, bf16[128,512]{1,0:T(8,128)(2,1)S(1)}, u32[]{:S(2)}, u32[]{:S(2)}) collective-permute-start(bf16[128,512]{1,0:T(8,128)(2,1)S(1)} %collective-permute-done.9.refs_3_), channel_id=1, source_target_pairs={{0,1},{1,0},{2,3},{3,2},{4,5},{5,4},{6,7},{7,6},{8,9},{9,8},{10,11... | collective-permute-start | bytes 393224 | tf_op jit(solution)/shard_map/ppermute | solution.py:534
  32.3 1.9 %collective-permute-start.8 = (bf16[128,512]{1,0:T(8,128)(2,1)S(1)}, bf16[128,512]{1,0:T(8,128)(2,1)S(1)}, u32[]{:S(2)}, u32[]{:S(2)}) collective-permute-start(bf16[128,512]{1,0:T(8,128)(2,1)S(1)} %collective-permute-done.refs_2_), channel_id=1, source_target_pairs={{0,1},{1,0},{2,3},{3,2},{4,5},{5,4},{6,7},{7,6},{8,9},{9,8},{10,11... | collective-permute-start | bytes 393224 | tf_op jit(solution)/shard_map/ppermute | solution.py:534
  34.3 4.4 %copy-start.6 = (bf16[2,512]{1,0:T(2,128)(2,1)S(1)}, bf16[2,512]{1,0:T(2,128)(2,1)}, u32[]{:S(2)}) copy-start(bf16[2,512]{1,0:T(2,128)(2,1)} %refs_4_.11) | copy-start | bytes 6148
  34.3 4.4 %copy-start.7 = (bf16[2,512]{1,0:T(2,128)(2,1)S(1)}, bf16[2,512]{1,0:T(2,128)(2,1)}, u32[]{:S(2)}) copy-start(bf16[2,512]{1,0:T(2,128)(2,1)} %refs_5_.11) | copy-start | bytes 6148
  34.3 4.4 %copy-start.8 = (f32[2,4]{1,0:T(2,128)S(1)}, f32[2,4]{1,0:T(2,128)}, u32[]{:S(2)}) copy-start(f32[2,4]{1,0:T(2,128)} %refs_6_.5) | copy-start | bytes 100
  35.1 6.4 %collective-permute-start.13 = (bf16[1,272,128]{2,1,0:T(8,128)(2,1)S(1)}, bf16[1,272,128]{2,1,0:T(8,128)(2,1)S(1)}, u32[]{:S(2)}, u32[]{:S(2)}) collective-permute-start(bf16[1,272,128]{2,1,0:T(8,128)(2,1)S(1)} %get-tuple-element.56), channel_id=1, source_target_pairs={{0,8},{8,0},{16,24},{24,16},{1,9},{9,1},{17,25},{25,17},{2,10},{10... | collective-permute-start | bytes 208904 | tf_op jit(solution)/shard_map/ppermute | solution.py:537
  36.6 4.9 %collective-permute-start.14 = (bf16[1,272,128]{2,1,0:T(8,128)(2,1)S(1)}, bf16[1,272,128]{2,1,0:T(8,128)(2,1)S(1)}, u32[]{:S(2)}, u32[]{:S(2)}) collective-permute-start(bf16[1,272,128]{2,1,0:T(8,128)(2,1)S(1)} %get-tuple-element.57), channel_id=1, source_target_pairs={{0,16},{8,24},{16,0},{24,8},{1,17},{9,25},{17,1},{25,9},{2,18},{10... | collective-permute-start | bytes 208904 | tf_op jit(solution)/shard_map/ppermute | solution.py:537
  38.1 5.2 %collective-permute-start.15 = (bf16[1,272,128]{2,1,0:T(8,128)(2,1)S(1)}, bf16[1,272,128]{2,1,0:T(8,128)(2,1)S(1)}, u32[]{:S(2)}, u32[]{:S(2)}) collective-permute-start(bf16[1,272,128]{2,1,0:T(8,128)(2,1)S(1)} %get-tuple-element.58), channel_id=1, source_target_pairs={{0,24},{8,16},{16,8},{24,0},{1,25},{9,17},{17,9},{25,1},{2,26},{10... | collective-permute-start | bytes 208904 | tf_op jit(solution)/shard_map/ppermute | solution.py:537
  46.0 3.9 %collective-permute-start.19 = (bf16[2,1,48,128]{3,2,1,0:T(8,128)(2,1)S(1)}, bf16[2,1,48,128]{3,2,1,0:T(8,128)(2,1)S(1)}, u32[]{:S(2)}, u32[]{:S(2)}) collective-permute-start(bf16[2,1,48,128]{3,2,1,0:T(8,128)(2,1)S(1)} %get-tuple-element.65), channel_id=1, source_target_pairs={{0,8},{8,0},{16,24},{24,16},{1,9},{9,1},{17,25},{25,17},{2,10},{10... | collective-permute-start | bytes 73736 | tf_op jit(solution)/shard_map/ppermute | solution.py:537
  46.6 3.8 %collective-permute-start.20 = (bf16[2,1,48,128]{3,2,1,0:T(8,128)(2,1)S(1)}, bf16[2,1,48,128]{3,2,1,0:T(8,128)(2,1)S(1)}, u32[]{:S(2)}, u32[]{:S(2)}) collective-permute-start(bf16[2,1,48,128]{3,2,1,0:T(8,128)(2,1)S(1)} %get-tuple-element.66), channel_id=1, source_target_pairs={{0,16},{8,24},{16,0},{24,8},{1,17},{9,25},{17,1},{25,9},{2,18},{10... | collective-permute-start | bytes 73736 | tf_op jit(solution)/shard_map/ppermute | solution.py:537
  47.2 4.7 %collective-permute-start.21 = (bf16[2,1,48,128]{3,2,1,0:T(8,128)(2,1)S(1)}, bf16[2,1,48,128]{3,2,1,0:T(8,128)(2,1)S(1)}, u32[]{:S(2)}, u32[]{:S(2)}) collective-permute-start(bf16[2,1,48,128]{3,2,1,0:T(8,128)(2,1)S(1)} %get-tuple-element.67), channel_id=1, source_target_pairs={{0,24},{8,16},{16,8},{24,0},{1,25},{9,17},{17,9},{25,1},{2,26},{10... | collective-permute-start | bytes 73736 | tf_op jit(solution)/shard_map/ppermute | solution.py:537
